TPU v7x, 256 devices: a 4x2x16 block of a 4x16x16 slice. The times are simulated.
256 devices in a mesh: grp: 2 (over y), fs: 32 (over z, core), tp: 4 (over x).
Axes of the slice: x: 4, y: 2, z: 16, core: 2. Of those that a mesh axis runs over, the one named last changes fastest.
The devices are a block of a 4x16x16 slice.
Arguments:
- tokens: bfloat16 [4096, 2048], P(('grp', 'fs')), parts along dimension 0, may hold values from -6 to 6
- routes: int32 [4096, 2], P(('grp', 'fs')), parts along dimension 0, may hold values from 0 to 3, as said below
- route_logits: float32 [4096, 2], P(('grp', 'fs')), parts along dimension 0, may hold values from -8 to 8
- gain: float32 [2048], P('fs'), may hold values from 0.1 to 1.9
- w_gate: float32 [4, 2048, 7168], P(None, 'fs', 'tp'), may hold values from -0.125 to 0.125
- w_up: float32 [4, 2048, 7168], P(None, 'fs', 'tp'), may hold values from -0.125 to 0.125
- w_down: float32 [4, 7168, 2048], P(None, 'fs', 'tp'), may hold values from -0.0625 to 0.0625
Outputs:
- gate_served: bfloat16 [8, 2048, 7168], P(('grp', 'tp'), None, 'fs'), parts along dimension 0
- up_served: bfloat16 [8, 2048, 7168], P(('grp', 'tp'), None, 'fs'), parts along dimension 0
- down_served: bfloat16 [8, 7168, 2048], P(('grp', 'tp'), 'fs'), parts along dimension 0
- mixed: bfloat16 [4096, 2048], P(('grp', 'fs'), 'tp'), parts along dimension 0
There are 2 independent parts, one for each index of `grp`. A program takes and returns all parts, laid end to end along the dimension named above; an argument that names none is the same for every part. Nothing has to cross between parts.
Inputs may be any that keep to these rules, and one draw needn't show every extreme that they name: `routes`: each row names 2 different experts; every expert is named by some row.
All inputs are finite; a program needn't handle non-finite values.
Results may differ from a plain program's by a relative error of at most 0.0085.
Values may be sent and summed in bfloat16 or wider, within the bound.
A program may use at most 128 MiB of HBM per device.

v0:
```python
import jax
import jax.numpy as jnp
from jax import lax
from jax.sharding import PartitionSpec as P


def sent_together(arrays, axis, split_dim, concat_dim, along):
    ends, at = ([], 0)
    for a in arrays[:-1]:
        at += a.shape[along]
        ends.append(at)
    both = jnp.concatenate(arrays, axis=along)
    return tuple(
        jnp.split(
            lax.all_to_all(both, axis, split_axis=split_dim, concat_axis=concat_dim, tiled=True),
            ends,
            axis=along,
        )
    )


def sent_together_2(arrays, axis, dim, along):
    columns = [a.reshape(*a.shape[:along], -1) for a in arrays]
    both = jnp.concatenate(columns, axis=along)
    out, at, gathered = (lax.all_gather(both, axis, axis=dim, tiled=True), 0, [])
    for a, column in zip(arrays, columns):
        piece = out[..., at : at + column.shape[along]]
        gathered.append(piece.reshape(*piece.shape[:along], *a.shape[along:]))
        at += column.shape[along]
    return tuple(gathered)


def cut_along(array, dim, count):
    dims = array.shape
    tiles = array.reshape(*dims[:dim], count, dims[dim] // count, *dims[dim + 1 :])
    return jnp.moveaxis(tiles, dim, 0)


def sent_and_summed(array, axis, dim):
    count = lax.axis_size(axis)
    tiles = lax.all_to_all(cut_along(array, dim, count), axis, 0, 0, tiled=True)
    return jnp.sum(tiles, axis=0)


def body(tokens, routes, route_logits, gain, w_gate, w_up, w_down):
    gate_cast = (w_gate * gain[None, :, None]).astype(jnp.bfloat16)
    up_cast = (w_up * gain[None, :, None]).astype(jnp.bfloat16)
    down_cast = w_down.astype(jnp.bfloat16)
    gate_tp, up_tp, down_served = (
        lax.all_to_all(gate_cast, "tp", split_axis=0, concat_axis=2, tiled=True),
        lax.all_to_all(up_cast, "tp", split_axis=0, concat_axis=2, tiled=True),
        lax.all_to_all(down_cast, "tp", split_axis=0, concat_axis=2, tiled=True),
    )
    gate_served, up_served = sent_together((gate_tp, up_tp), "fs", 2, 1, 0)
    values = tokens.astype(jnp.float32)
    mean_square = jnp.mean(values * values, axis=-1, keepdims=True)
    normed = (values * lax.rsqrt(mean_square + 1e-06)).astype(jnp.bfloat16)
    expert_id = lax.axis_index("tp")
    first = jax.nn.sigmoid(route_logits[:, 0] - route_logits[:, 1])
    second = jax.nn.sigmoid(route_logits[:, 1] - route_logits[:, 0])
    weight_col = first * (routes[:, 0] == expert_id).astype(jnp.float32)
    weight_col = (weight_col + second * (routes[:, 1] == expert_id).astype(jnp.float32)).astype(
        jnp.bfloat16
    )
    gate_local = gate_served[0]
    up_local = up_served[0]
    piece_rows, piece_weight = sent_together_2((normed, weight_col), "fs", 0, 1)
    gate_act = jnp.dot(piece_rows, gate_local, preferred_element_type=jnp.float32)
    up_act = jnp.dot(piece_rows, up_local, preferred_element_type=jnp.float32)
    hidden_rows = jax.nn.silu(gate_act) * up_act * piece_weight[:, None].astype(jnp.float32)
    hidden = hidden_rows.astype(jnp.bfloat16)
    down_local = down_served[0]
    summed_rows = lax.psum_scatter(
        jnp.dot(hidden, down_local, preferred_element_type=jnp.float32),
        "fs",
        scatter_dimension=0,
        tiled=True,
    )
    mixed = sent_and_summed(summed_rows, "tp", 1)
    return (gate_served, up_served, down_served, mixed.astype(jnp.bfloat16))


def solution(mesh):
    return jax.shard_map(
        body,
        mesh=mesh,
        in_specs=(
            P(("grp", "fs"), None),
            P(("grp", "fs"), None),
            P(("grp", "fs"), None),
            P("fs"),
            P(None, "fs", "tp"),
            P(None, "fs", "tp"),
            P(None, "fs", "tp"),
        ),
        out_specs=(
            P(("grp", "tp"), None, "fs"),
            P(("grp", "tp"), None, "fs"),
            P(("grp", "tp"), "fs", None),
            P(("grp", "fs"), "tp"),
        ),
        check_vma=False,
    )
```

profile of v0, /device:TPU:33, one launch (start us, length us, event | category | flops | bytes accessed | tf_op | source)
XLA Modules:
  0.0 360.2 jit_solution(13875330566022918010)
XLA Ops:
  7.2 1.1 fusion.23
  8.4 1.1 fusion.24
  9.4 0.8 fusion.26
  10.3 0.7 pad_maximum_fusion.1
  11.1 3.3 multiply_convert_fusion.1
  14.5 13.9 %all_to_all.74 = bf16[4,64,1792]{2,1,0:T(8,128)(2,1)S(1)} all-to-all(bf16[4,64,1792]{2,1,0:T(8,128)(2,1)S(1)} %get-tuple-element.14), channel_id=1, replica_groups=mesh['grp'=2,'fs'=32,'tp'=4] {'tp'}, dimensions={0} | all-to-all | bytes 1835008 | tf_op jit(solution)/shard_map/all_to_all | solution.py:50
  28.4 3.6 all-to-all-start.1
  32.0 2.5 convert_element_type.30
  34.6 1.0 copy.40
  35.6 5.4 %all-to-all-done.1 = bf16[4,64,1792]{2,1,0:T(8,128)(2,1)S(1)} async-done(((bf16[4,64,1792]{2,1,0:T(8,128)(2,1)}), bf16[4,64,1792]{2,1,0:T(8,128)(2,1)S(1)}, u32[]{:S(2)}, u32[]{:S(2)}) %all-to-all-start.1) | async-done | bytes 917536 | tf_op jit(solution)/shard_map/all_to_all | solution.py:51
  41.0 3.6 all-to-all-start.3
  44.7 1.1 copy-done
  45.9 6.1 %copy.26 = bf16[2,64,7168]{1,0,2:T(2,128)(2,1)} copy(bf16[2,64,7168]{2,1,0:T(8,128)(2,1)S(1)} %pad_maximum_fusion) | data formatting | bytes 3670016 | tf_op jit(solution)/shard_map/concatenate | solution.py:12
  52.1 8.8 %reshape.29 = bf16[32,2,14336]{2,1,0:T(2,128)(2,1)} reshape(bf16[7168,2,64]{2,1,0:T(2,128)(2,1)} %bitcast.36) | data formatting | bytes 3670016
  60.9 33.4 %all-to-all-start.2 = ((bf16[32,2,14336]{2,1,0:T(2,128)(2,1)}), bf16[32,2,14336]{2,1,0:T(2,128)(2,1)S(1)}, u32[]{:S(2)}, u32[]{:S(2)}) async-start(bf16[32,2,14336]{2,1,0:T(2,128)(2,1)} %reshape.29), calls=%async_computation.2 | async-start | bytes 3670016 | tf_op jit(solution)/shard_map/all_to_all | solution.py:15
  94.5 0.7 copy.30
  95.3 1.1 copy.43
  96.4 84.4 %all-to-all-done.2 = bf16[32,2,14336]{2,1,0:T(2,128)(2,1)S(1)} async-done(((bf16[32,2,14336]{2,1,0:T(2,128)(2,1)}), bf16[32,2,14336]{2,1,0:T(2,128)(2,1)S(1)}, u32[]{:S(2)}, u32[]{:S(2)}) %all-to-all-start.2) | async-done | bytes 1835040 | tf_op jit(solution)/shard_map/all_to_all | solution.py:15
  180.8 3.7 %reshape.30 = bf16[7168,2,64]{2,1,0:T(2,128)(2,1)} reshape(bf16[32,2,14336]{2,1,0:T(2,128)(2,1)S(1)} %all-to-all-done.2) | data formatting | bytes 3670016
  184.5 6.3 %copy.38 = bf16[2,64,32,224]{3,2,1,0:T(8,128)(2,1)S(1)} copy(bf16[2,64,32,224]{1,0,3,2:T(2,128)(2,1)} %bitcast.37) | data formatting | bytes 3670016 | tf_op jit(solution)/shard_map/all_to_all | solution.py:15
  191.5 0.6 copy.29
  192.1 1.3 convert_reduce_fusion
  193.4 7.5 %fusion.2 = f32[2048,224]{0,1:T(8,128)} fusion(bf16[2048,224]{1,0:T(8,128)(2,1)S(1)} %bitcast.43, bf16[2048,2049]{1,0:T(8,128)(2,1)} %all-gather.2.cloned.1.call-done), kind=kOutput, calls=%fused_computation.2 | convolution fusion | flops 1879048192 | bytes 11141120 | tf_op jit(solution)/shard_map/dot_general | solution.py:68
  200.9 11.4 %fusion.14 = f32[2048,2048]{1,0:T(8,128)} fusion(bf16[224,2048]{1,0:T(8,128)(2,1)} %bitcast.50, bf16[2048,224]{1,0:T(8,128)(2,1)S(1)} %bitcast.38, bf16[2048,2049]{1,0:T(8,128)(2,1)} %all-gather.2.cloned.1.call-done, f32[2048,224]{0,1:T(8,128)} %fusion.2, f32[2048]{0:T(1024)S(1)} %convert_reduce_fusion), kind=kOutput, calls=%fused_computation.7 | convolution fusion | flops 3761307648 | bytes 28844032 | tf_op jit(solution)/shard_map/dot_general | solution.py:74
  212.3 127.5 %reduce-scatter.2.cloned.1.call-done = f32[64,2048]{1,0:T(8,128)} async-done(((f32[2048,2048]{1,0:T(8,128)}), f32[64,2048]{1,0:T(8,128)}) %reduce-scatter.2.cloned.1.call-update) | async-done | bytes 524304 | tf_op jit(solution)/shard_map/reduce_scatter | solution.py:73
  339.8 1.9 copy.45
  341.7 4.1 %all-to-all-start.4 = ((f32[4,64,512]{2,1,0:T(8,128)}), f32[4,64,512]{2,1,0:T(8,128)S(1)}, u32[]{:S(2)}, u32[]{:S(2)}) async-start(f32[4,64,512]{2,1,0:T(8,128)} %bitcast.51), calls=%async_computation.5 | async-start | bytes 1048576 | tf_op jit(solution)/shard_map/all_to_all | solution.py:41
  345.7 1.0 copy.42
  346.8 1.3 copy.36
  348.1 1.3 copy.37
  349.3 3.4 all-to-all-done.4
  352.7 0.7 reduce_sum.19
  (13 shorter events, 1.6 us)
Async XLA Ops:
  7.2 184.9 %all-gather.2.cloned.1.call-start = ((), (), s32[]{:S(2)}) async-start(), calls=%async_computation.6 | async-start | bytes 9191424 | tf_op jit(solution)/shard_map/all_gather | solution.py:25
  28.4 12.5 %all-to-all-start.1 = ((bf16[4,64,1792]{2,1,0:T(8,128)(2,1)}), bf16[4,64,1792]{2,1,0:T(8,128)(2,1)S(1)}, u32[]{:S(2)}, u32[]{:S(2)}) async-start(bf16[4,64,1792]{2,1,0:T(8,128)(2,1)} %get-tuple-element.15), calls=%async_computation.1 | async-start | bytes 1835008 | tf_op jit(solution)/shard_map/all_to_all | solution.py:51
  41.0 19.9 %all-to-all-start.3 = ((bf16[4,224,512]{2,1,0:T(8,128)(2,1)}), bf16[4,224,512]{2,1,0:T(8,128)(2,1)S(1)}, u32[]{:S(2)}, u32[]{:S(2)}) async-start(bf16[4,224,512]{2,1,0:T(8,128)(2,1)} %convert_element_type.30), calls=%async_computation.3 | async-start | bytes 1835008 | tf_op jit(solution)/shard_map/all_to_all | solution.py:52
  44.6 1.2 copy-start
  60.9 119.9 %all-to-all-start.2 = ((bf16[32,2,14336]{2,1,0:T(2,128)(2,1)}), bf16[32,2,14336]{2,1,0:T(2,128)(2,1)S(1)}, u32[]{:S(2)}, u32[]{:S(2)}) async-start(bf16[32,2,14336]{2,1,0:T(2,128)(2,1)} %reshape.29), calls=%async_computation.2 | async-start | bytes 3670016 | tf_op jit(solution)/shard_map/all_to_all | solution.py:15
  94.3 245.5 %reduce-scatter.2.cloned.1.call-start = ((), (), s32[]{:S(2)}) async-start(), calls=%async_computation.7 | async-start | bytes 17301504 | tf_op jit(solution)/shard_map/reduce_scatter | solution.py:73
  341.7 11.0 %all-to-all-start.4 = ((f32[4,64,512]{2,1,0:T(8,128)}), f32[4,64,512]{2,1,0:T(8,128)S(1)}, u32[]{:S(2)}, u32[]{:S(2)}) async-start(f32[4,64,512]{2,1,0:T(8,128)} %bitcast.51), calls=%async_computation.5 | async-start | bytes 1048576 | tf_op jit(solution)/shard_map/all_to_all | solution.py:41
Sparse Core Ops, SparseCore 0:
  11.3 105.6 all-gather.1
  212.4 127.3 reduce-scatter.1
where the time goes:
time: 364 us; the launch traced here: 360 us
  waiting for transfers between devices  221 us (61%)
  starting transfers between devices  45 us (12%)
  local copies, waits for them, and re-layouts  35.8 us (10%)
  matrix products  18.9 us (5%)
  between operations  14.2 us (4%)
  blocking collectives  13.9 us (4%)
  other arithmetic  11.7 us (3%)
    reduce_scatter x1, waiting for transfers between devices, body(): lax.psum_scatter(jnp.dot(hidden, down_local, preferred_element_type=jnp.f...  127 us
    all_to_all x1, waiting for transfers between devices, sent_together(): lax.all_to_all(both, axis, split_axis=split_dim, concat_axis=concat_dim,...  84.4 us
    all_to_all x1, starting transfers between devices, sent_together(): lax.all_to_all(both, axis, split_axis=split_dim, concat_axis=concat_dim,...  33.4 us
    unnamed x7, local copies, waits for them, and re-layouts  17.3 us
    all_to_all x1, blocking collectives, body(): lax.all_to_all(gate_cast, 'tp', split_axis=0, concat_axis=2, tiled=True)  13.9 us
    dot_general x1, matrix products, body(): jnp.dot(hidden, down_local, preferred_element_type=jnp.float32)  11.4 us
    dot_general x1, matrix products, body(): jnp.dot(piece_rows, gate_local, preferred_element_type=jnp.float32)  7.47 us
  transfers between devices with their start and end apart: 6, of which 4 were waited for; matrix products, arithmetic and copies ran while one was open for 11% of the time, Pallas kernels for 0%

commit v1 on v0

v1 whole, which is shorter than its diff:
```python
import functools

import jax
import jax.numpy as jnp
from jax import lax
from jax.experimental import pallas as pl
from jax.experimental.pallas import tpu as pltpu
from jax.sharding import PartitionSpec as P

MESH = pl.DeviceIdType.MESH
DMA = pltpu.SemaphoreType.DMA
LANES = 128


def remote(src, dst, send, recv, **where):
    return pltpu.make_async_remote_copy(
        src_ref=src, dst_ref=dst, send_sem=send, recv_sem=recv, device_id=where, device_id_type=MESH
    )


def hand_over(
    FS, TP, wp, dn, nt, wt, gu, ds, tok, wall, xr,
    xw_s, xw_r, xd_s, xd_r, loc, wt_s, wt_r, rs, rr, xt_s, xt_r, xo_s, xo_r,
    cc_s, cc_r, za_s, za_r, y_s, y_r, yd_s, yd_r,
):
    Z = FS // 2
    H = Z // 2
    x, f, g = lax.axis_index("tp"), lax.axis_index("fs"), lax.axis_index("grp")
    z, c = f // 2, f % 2
    p = g % 2
    mate = g + 1 - 2 * p
    slices = wp.shape[1]
    fb = nt.shape[1] // TP
    half = nt.shape[0] // 2
    db = dn.shape[2]

    def cols(i):
        return pl.ds(pl.multiple_of(i * fb, LANES), fb)

    def dcols(i):
        return pl.ds(pl.multiple_of(i * db, LANES), db)

    barrier = pltpu.get_barrier_semaphore()

    def greet(r, _):
        pl.semaphore_signal(barrier, inc=1, device_id={"fs": (f + r) % FS}, device_id_type=MESH)
        return 0

    lax.fori_loop(1, FS, greet, 0)
    for k in range(1, TP):
        pl.semaphore_signal(barrier, inc=1, device_id={"tp": (x + k) % TP}, device_id_type=MESH)
    pl.semaphore_signal(barrier, inc=1, device_id={"grp": mate}, device_id_type=MESH)
    pl.semaphore_wait(barrier, FS - 1 + TP - 1 + 1)

    def ring(i, fo, side):
        to = ((z + 1) % Z if side == 0 else (z + Z - 1) % Z) * 2 + c
        return remote(tok.at[fo, :, cols(x)], tok.at[fo, :, cols(x)], rs.at[side, i], rr.at[side, i], fs=to)

    def ring_first(side):
        to = ((z + 1) % Z if side == 0 else (z + Z - 1) % Z) * 2 + c
        return remote(nt.at[:, cols(x)], tok.at[f, :, cols(x)], rs.at[side, 0], rr.at[side, 0], fs=to)

    ring_first(0).start()
    ring_first(1).start()
    other = f + 1 - 2 * c
    own_cross = remote(nt, tok.at[f], cc_s.at[Z - 1], cc_r.at[Z - 1], fs=other)
    own_cross.start()

    def xw(k):
        return remote(wp.at[(x + k) % TP], xr.at[x], xw_s.at[k - 1], xw_r.at[k - 1], tp=(x + k) % TP)

    def xd(k):
        return remote(dn.at[(x + k) % TP], ds.at[p, :, dcols(x)], xd_s.at[k - 1], xd_r.at[k - 1], tp=(x + k) % TP)

    for k in (2, 1, 3):
        xw(k).start()
    for k in (2, 1, 3):
        xd(k).start()
    local = [
        pltpu.make_async_copy(wp.at[x], xr.at[x], loc.at[0]),
        pltpu.make_async_copy(dn.at[x], ds.at[p, :, dcols(x)], loc.at[1]),
        pltpu.make_async_copy(nt, tok.at[f], loc.at[2]),
        pltpu.make_async_copy(wt, wall.at[f], loc.at[3]),
    ]
    for copy in local:
        copy.start()

    def tell(r, _):
        remote(wt, wall.at[f], wt_s, wt_r, fs=(f + r) % FS).start()
        return 0

    lax.fori_loop(1, FS, tell, 0)

    def across(i, fo, side):
        to = (x + 1) % TP if side == 0 else (x + TP - 1) % TP
        return remote(tok.at[fo, :, cols(x)], tok.at[fo, :, cols(x)], xt_s.at[side, i], xt_r.at[side, i], tp=to)

    def from_left(s):
        return ((z + Z - s) % Z) * 2 + c

    def from_right(s):
        return ((z + s) % Z) * 2 + c

    def ring_step(s, _):
        fo = from_left(s)
        ring(s - 1, fo, 0).wait_recv()
        ring(s, fo, 0).start()
        fo2 = from_right(s)
        ring(s - 1, fo2, 1).wait_recv()

        @pl.when(s < H - 1)
        def _():
            ring(s, fo2, 1).start()

        for side in (0, 1):
            across(2 * s - 2, fo, side).start()
            across(2 * s - 1, fo2, side).start()
        return 0

    lax.fori_loop(1, H, ring_step, 0)
    last = from_left(H)
    ring(H - 1, last, 0).wait_recv()
    for side in (0, 1):
        across(2 * H - 2, last, side).start()

    for copy in local:
        copy.wait()
    for k in (2, 1, 3):
        xw(k).wait_recv()

    def apart(i):
        m = H - 1 - (i - 1) // 2
        return jnp.where(i == 0, H, jnp.where(i % 2 == 1, m, Z - m))

    def za(d, cd):
        to = ((z + d) % Z) * 2 + cd
        return remote(
            xr.at[to // slices, to % slices], gu.at[:, f, p], za_s.at[d, cd], za_r.at[d, c], fs=to
        )

    def za_recv(d, cs):
        fo = ((z + Z - d) % Z) * 2 + cs
        return remote(xr.at[0, 0], gu.at[:, fo, p], za_s.at[d, cs], za_r.at[d, cs], fs=other)

    def za_start(i, _):
        d = apart(i)
        za(d, 0).start()
        za(d, 1).start()
        return 0

    lax.fori_loop(0, Z - 1, za_start, 0)
    za(0, 1 - c).start()
    own = pltpu.make_async_copy(xr.at[f // slices, f % slices], gu.at[:, f, p], loc.at[4])
    own.start()

    for k in (2, 1, 3):
        xd(k).wait_recv()
    yd = remote(ds.at[p], ds.at[p], yd_s, yd_r, grp=mate)
    yd.start()

    def y_hand(d):
        zo = (z + Z - d) % Z
        part = gu.at[:, pl.ds(2 * zo, 2), p]
        return remote(part, part, y_s.at[d], y_r.at[d], grp=mate)

    def origin(i):
        s = i // 2 + 1
        return jnp.where(i % 2 == 0, from_left(s), from_right(s))

    def onward(i, fo, side):
        to = (x + 1) % TP if side == 0 else (x + TP - 1) % TP
        held = (x + TP - 1) % TP if side == 0 else (x + 1) % TP
        part = tok.at[fo, pl.ds(side * half, half), cols(held)]
        return remote(part, part, xo_s.at[side, i], xo_r.at[side, i], tp=to)

    def cross(i, fo):
        return remote(tok.at[fo], tok.at[fo], cc_s.at[i], cc_r.at[i], fs=other)

    def finish(i):
        fo = origin(i)
        for side in (0, 1):
            onward(i, fo, side).wait_recv()
        cross(i, fo).start()

    def flow(i, _):
        fo = origin(i)
        for side in (0, 1):
            across(i, fo, side).wait_recv()
            onward(i, fo, side).start()
        d = apart(i)
        za_recv(d, 0).wait_recv()
        za_recv(d, 1).wait_recv()
        y_hand(d).start()

        @pl.when(i > 0)
        def _():
            finish(i - 1)

        return 0

    lax.fori_loop(0, Z - 1, flow, 0)
    own.wait()
    za_recv(0, 1 - c).wait_recv()
    y_hand(0).start()
    finish(Z - 2)

    def drain(i, _):
        fo = origin(i)
        for side in (0, 1):
            across(i, fo, side).wait_send()
            onward(i, fo, side).wait_send()
        cross(i, fo).wait()
        d = apart(i)
        za(d, 0).wait_send()
        za(d, 1).wait_send()
        y_hand(d).wait()
        return 0

    lax.fori_loop(0, Z - 1, drain, 0)

    def ring_drain(s, _):
        ring(s, f, 0).wait_send()

        @pl.when(s < H - 1)
        def _():
            ring(s, f, 1).wait_send()

        return 0

    lax.fori_loop(0, H, ring_drain, 0)
    own_cross.wait()
    za(0, 1 - c).wait_send()
    y_hand(0).wait()
    yd.wait()
    for k in (1, 2, 3):
        xw(k).wait_send()
        xd(k).wait_send()
    tiles = remote(wall.at[pl.ds(0, FS - 1)], wall.at[pl.ds(0, FS - 1)], wt_s, wt_r, fs=other)
    tiles.wait_send()
    tiles.wait_recv()


def run_hand_over(FS, TP, wp, dn, nt, wt):
    Z = FS // 2
    _, slices, two, half, ff = wp.shape
    vmem = pl.BlockSpec(memory_space=pltpu.VMEM)
    hbm = pl.BlockSpec(memory_space=pl.ANY)
    return pl.pallas_call(
        functools.partial(hand_over, FS, TP),
        out_shape=(
            jax.ShapeDtypeStruct((two, FS, 2, half, ff), jnp.bfloat16),
            jax.ShapeDtypeStruct((2, dn.shape[1], TP * dn.shape[2]), jnp.bfloat16),
            jax.ShapeDtypeStruct((FS,) + nt.shape, jnp.bfloat16),
            jax.ShapeDtypeStruct((FS,) + wt.shape, jnp.bfloat16),
        ),
        in_specs=[vmem] * 4,
        out_specs=(hbm, hbm, hbm, vmem),
        scratch_shapes=[
            pltpu.VMEM(wp.shape, jnp.bfloat16),
            DMA((TP - 1,)), DMA((TP - 1,)), DMA((TP - 1,)), DMA((TP - 1,)),
            DMA((5,)), DMA, DMA,
            DMA((2, Z // 2)), DMA((2, Z // 2)),
            DMA((2, Z - 1)), DMA((2, Z - 1)), DMA((2, Z - 1)), DMA((2, Z - 1)),
            DMA((Z,)), DMA((Z,)),
            DMA((Z, 2)), DMA((Z, 2)),
            DMA((Z,)), DMA((Z,)), DMA, DMA,
        ],
        compiler_params=pltpu.CompilerParams(collective_id=0, has_side_effects=True, vmem_limit_bytes=32 << 20),
        cost_estimate=pl.CostEstimate(flops=10**9, bytes_accessed=30 << 20, transcendentals=0),
        name="hand_over",
    )(wp, dn, nt, wt)


def body(FS, TP, tokens, routes, route_logits, gain, w_gate, w_up, w_down):
    p = lax.axis_index("grp") % 2
    e = lax.axis_index("tp")
    rows, ff = w_gate.shape[1:]
    slices = FS // TP
    half = rows // 2

    def mine(w):
        part = lax.dynamic_slice_in_dim(w, p * half, half, 1)
        scale = lax.dynamic_slice_in_dim(gain, p * half, half, 0)
        part = (part * scale[None, :, None]).astype(jnp.bfloat16)
        return part.reshape(TP, half, slices, ff // slices).transpose(0, 2, 1, 3)

    wp = jnp.stack([mine(w_gate), mine(w_up)], axis=2)
    hrows = w_down.shape[1] // 2
    dn = lax.dynamic_slice_in_dim(w_down, p * hrows, hrows, 1).astype(jnp.bfloat16)

    values = tokens.astype(jnp.float32)
    mean_square = jnp.mean(values * values, axis=-1, keepdims=True)
    nt = (values * lax.rsqrt(mean_square + 1e-06)).astype(jnp.bfloat16)
    first = jax.nn.sigmoid(route_logits[:, 0] - route_logits[:, 1])
    second = jax.nn.sigmoid(route_logits[:, 1] - route_logits[:, 0])
    weight = first * (routes[:, 0] == e).astype(jnp.float32)
    weight = (weight + second * (routes[:, 1] == e).astype(jnp.float32)).astype(jnp.bfloat16)
    count = weight.shape[0]
    wt = jnp.broadcast_to(jnp.pad(weight, (0, LANES - count))[None], (16, LANES))

    gu, ds, tok, wall = run_hand_over(FS, TP, wp, dn, nt, wt)
    gate_served = gu[0].reshape(1, FS * rows, ff // slices)
    up_served = gu[1].reshape(1, FS * rows, ff // slices)
    down_served = ds.reshape(1, 2 * hrows, TP * dn.shape[2])
    x_all = tok.reshape(FS * count, -1)
    w_all = wall[:, 0, :count].reshape(FS * count)

    contract = (((0,), (1,)), ((), ()))
    gate_act = lax.dot_general(gate_served[0], x_all, contract, preferred_element_type=jnp.float32)
    up_act = lax.dot_general(up_served[0], x_all, contract, preferred_element_type=jnp.float32)
    hidden = (jax.nn.silu(gate_act) * up_act * w_all[None, :].astype(jnp.float32)).astype(jnp.bfloat16)
    every = lax.all_gather(hidden, "tp", axis=0, tiled=True)
    down = w_down.astype(jnp.bfloat16).reshape(-1, w_down.shape[2])
    part = lax.dot_general(every, down, (((0,), (0,)), ((), ())), preferred_element_type=jnp.float32)
    mixed = lax.psum_scatter(part, "fs", scatter_dimension=0, tiled=True)
    return (gate_served, up_served, down_served, mixed.astype(jnp.bfloat16))


def solution(mesh):
    return jax.shard_map(
        functools.partial(body, mesh.shape["fs"], mesh.shape["tp"]),
        mesh=mesh,
        in_specs=(
            P(("grp", "fs"), None),
            P(("grp", "fs"), None),
            P(("grp", "fs"), None),
            P("fs"),
            P(None, "fs", "tp"),
            P(None, "fs", "tp"),
            P(None, "fs", "tp"),
        ),
        out_specs=(
            P(("grp", "tp"), None, "fs"),
            P(("grp", "tp"), None, "fs"),
            P(("grp", "tp"), "fs", None),
            P(("grp", "fs"), "tp"),
        ),
        check_vma=False,
    )
```

time: 364 us -> 321 us (0.88)
  Pallas kernels: 0 us -> 120 us
  waiting for transfers between devices: 221 us -> 152 us
  starting transfers between devices: 45 us -> 0.31 us
  local copies, waits for them, and re-layouts: 35.8 us -> 10.7 us
  blocking collectives: 13.9 us -> 0 us
  other arithmetic: 11.7 us -> 6.28 us
    pallas_call x0 -> x1, Pallas kernels: none -> 120 us  [run_hand_over(): pl.pallas_call(functools.partial(hand_over, FS, TP), out_shape=(jax.Shape...]
    all_to_all x4 -> x0, waiting for transfers between devices: 93.1 us -> none  [the longest x1 84.4 us: sent_together(): lax.all_to_all(both, axis, split_axis=split_dim, concat_axis=concat_dim,...]
    all_to_all x4 -> x0, starting transfers between devices: 44.7 us -> none  [the longest x1 33.4 us: sent_together(): lax.all_to_all(both, axis, split_axis=split_dim, concat_axis=concat_dim,...]
    all_gather x1, waiting for transfers between devices: 0.02 us -> 42.6 us  [body(): every = lax.all_gather(hidden, 'tp', axis=0, tiled=True)]
    reduce_scatter x1, waiting for transfers between devices: 127 us -> 109 us  [body(): mixed = lax.psum_scatter(part, 'fs', scatter_dimension=0, tiled=True)]
    all_to_all x1 -> x0, blocking collectives: 13.9 us -> none  [body(): lax.all_to_all(gate_cast, 'tp', split_axis=0, concat_axis=2, tiled=True)]
    unnamed x7 -> x13, local copies, waits for them, and re-layouts: 17.3 us -> 6.69 us
    all_to_all x5 -> x0, local copies, waits for them, and re-layouts: 9.07 us -> none  [the longest x1 6.25 us: sent_together(): lax.all_to_all(both, axis, split_axis=split_dim, concat_axis=concat_dim,...]
  transfers between devices with their start and end apart: 6 -> 2, of which waited for: 4 -> 2; matrix products, arithmetic and copies ran while one was open for 11% -> 2% of each run, Pallas kernels for 0% -> 0%
where the time goes in v1:
time: 321 us; the launch traced here: 320 us
  waiting for transfers between devices  152 us (47%)
  Pallas kernels  120 us (37%)
  matrix products  16.7 us (5%)
  between operations  14.3 us (4%)
  local copies, waits for them, and re-layouts  10.7 us (3%)
  other arithmetic  6.28 us (2%)
    pallas_call x1, Pallas kernels, run_hand_over(): pl.pallas_call(functools.partial(hand_over, FS, TP), out_shape=(jax.Shape...  120 us
    reduce_scatter x1, waiting for transfers between devices, body(): mixed = lax.psum_scatter(part, 'fs', scatter_dimension=0, tiled=True)  109 us
    all_gather x1, waiting for transfers between devices, body(): every = lax.all_gather(hidden, 'tp', axis=0, tiled=True)  42.6 us
    unnamed x13, local copies, waits for them, and re-layouts  6.69 us
    dot_general x1, matrix products, body(): lax.dot_general(every, down, (((0,), (0,)), ((), ())), preferred_element_...  6.6 us
  transfers between devices with their start and end apart: 2, of which 2 were waited for; matrix products, arithmetic and copies ran while one was open for 2% of the time, Pallas kernels for 0%

profile of v1, /device:TPU:33, one launch (start us, length us, event | category | flops | bytes accessed | tf_op | source)
XLA Modules:
  0.0 319.7 jit_solution(2069296596326604736)
XLA Ops:
  7.2 0.1 all-gather.2.cloned.1.call-start
  7.3 0.7 dynamic_slice.14
  8.0 1.7 multiply_convert_fusion.1
  9.7 0.8 reshape.56
  10.5 0.8 reshape.57
  11.2 0.0 copy-done.2
  11.2 0.2 fusion.2
  11.4 0.1 fusion.3.nt
  11.5 0.3 copy_bitcast_fusion
  11.8 0.0 copy-start.3
  11.8 0.0 copy-start.4
  11.8 0.2 pad_maximum_fusion.wp
  12.0 1.2 dynamic-slice_convert_fusion.dn
  13.3 0.0 copy-done.3
  13.3 119.9 %hand_over.1 = (bf16[2,32,2,32,224]{4,3,2,1,0:T(8,128)(2,1)S(1)}, bf16[2,112,2048]{2,1,0:T(8,128)(2,1)S(1)}, bf16[32,64,2048]{2,1,0:T(8,128)(2,1)S(1)}, bf16[32,16,128]{2,1,0:T(8,128)(2,1)S(1)}) custom-call(bf16[4,8,2,32,224]{4,3,2,1,0:T(8,128)(2,1)S(1)} %pad_maximum_fusion.wp, bf16[4,112,512]{2,1,0:T(8,128)(2,1)S(1)} %dynamic-slice_convert_fusion.dn, ...), custom_call_target="tpu_custom_call" | custom-call | flops 1000000000 | bytes 31457280 | tf_op jit(solution)/shard_map/hand_over/pallas_call | solution.py:248
  133.3 0.0 copy-start
  133.3 3.2 %copy-done = bf16[32,64,2048]{2,1,0:T(8,128)(2,1)} copy-done((bf16[32,64,2048]{2,1,0:T(8,128)(2,1)}, bf16[32,64,2048]{2,1,0:T(8,128)(2,1)S(1)}, u32[]{:S(2)}) %copy-start) | copy-done | bytes 8388632
  136.5 0.2 fusion.5
  136.7 0.1 reshape.65
  136.8 6.2 %fusion.6 = f32[224,2048]{1,0:T(8,128)S(1)} fusion(bf16[2048,224]{1,0:T(8,128)(2,1)S(1)} %bitcast.28, bf16[2048,2048]{1,0:T(8,128)(2,1)} %bitcast.24), kind=kOutput, calls=%fused_computation.20 | convolution fusion | flops 1879048192 | bytes 11141120 | tf_op jit(solution)/shard_map/dot_general | solution.py:309
  143.0 3.9 %fusion.1 = bf16[224,2048]{1,0:T(8,128)(2,1)} fusion(bf16[2048,224]{1,0:T(8,128)(2,1)S(1)} %bitcast.26, bf16[2048,2048]{1,0:T(8,128)(2,1)S(1)} %bitcast.25, f32[224,2048]{1,0:T(8,128)S(1)} %fusion.6, f32[2048]{0:T(1024)S(1)} %reshape.65), kind=kOutput, calls=%fused_computation.2 | convolution fusion | flops 1882259456 | bytes 12066816 | tf_op jit(solution)/shard_map/dot_general | solution.py:310
  146.9 0.1 all-gather.2.cloned.1.call-update
  147.0 0.2 reduce-scatter.2.cloned.1.call-start
  147.2 2.5 convert_element_type.51
  149.7 42.6 %all-gather.2.cloned.1.call-done = bf16[896,2048]{1,0:T(8,128)(2,1)} async-done(((bf16[224,2048]{1,0:T(8,128)(2,1)}), bf16[896,2048]{1,0:T(8,128)(2,1)}) %all-gather.2.cloned.1.call-update) | async-done | bytes 3670032 | tf_op jit(solution)/shard_map/all_gather | solution.py:312
  192.4 6.6 %fusion.7 = f32[2048,512]{1,0:T(8,128)} fusion(bf16[896,2048]{1,0:T(8,128)(2,1)} %all-gather.2.cloned.1.call-done, bf16[896,512]{1,0:T(8,128)(2,1)} %bitcast.30), kind=kOutput, calls=%fused_computation.21 | convolution fusion | flops 1879048192 | bytes 8781824 | tf_op jit(solution)/shard_map/dot_general | solution.py:314
  199.0 0.1 reduce-scatter.2.cloned.1.call-update
  199.0 1.3 copy.15
  200.3 1.3 copy.16
  201.6 108.8 %reduce-scatter.2.cloned.1.call-done = f32[64,512]{1,0:T(8,128)} async-done(((f32[2048,512]{1,0:T(8,128)}), f32[64,512]{1,0:T(8,128)}) %reduce-scatter.2.cloned.1.call-update) | async-done | bytes 131088 | tf_op jit(solution)/shard_map/reduce_scatter | solution.py:315
  310.4 1.5 convert_element_type.52
  311.9 0.9 copy.20
  (9 shorter events, 0.1 us)
Async XLA Ops:
  7.2 185.2 %all-gather.2.cloned.1.call-start = ((), (), s32[]{:S(2)}) async-start(), calls=%async_computation.1 | async-start | bytes 4587520 | tf_op jit(solution)/shard_map/all_gather | solution.py:312
  8.0 3.2 %copy-start.2 = (bf16[64,2048]{1,0:T(8,128)(2,1)S(1)}, bf16[64,2048]{1,0:T(8,128)(2,1)}, u32[]{:S(2)}) copy-start(bf16[64,2048]{1,0:T(8,128)(2,1)} %param.7) | copy-start | bytes 786436
  11.8 1.5 copy-start.3
  11.8 1.5 copy-start.4
  133.3 3.2 %copy-start = (bf16[32,64,2048]{2,1,0:T(8,128)(2,1)}, bf16[32,64,2048]{2,1,0:T(8,128)(2,1)S(1)}, u32[]{:S(2)}) copy-start(bf16[32,64,2048]{2,1,0:T(8,128)(2,1)S(1)} %get-tuple-element.10) | copy-start | bytes 25165828
  136.8 6.2 %copy-start.1 = (bf16[32,64,2048]{2,1,0:T(8,128)(2,1)S(1)}, bf16[32,64,2048]{2,1,0:T(8,128)(2,1)}, u32[]{:S(2)}) copy-start(bf16[32,64,2048]{2,1,0:T(8,128)(2,1)} %copy-done) | copy-start | bytes 25165828
  147.0 163.4 %reduce-scatter.2.cloned.1.call-start = ((), (), s32[]{:S(2)}) async-start(), calls=%async_computation.2 | async-start | bytes 4325376 | tf_op jit(solution)/shard_map/reduce_scatter | solution.py:315
Sparse Core Ops, SparseCore 0:
  147.1 45.2 all-gather.1
  199.2 111.1 reduce-scatter.1

commit v2 on v1

--- a/solution.py
+++ b/solution.py
@@ -271,6 +271,171 @@
     )(wp, dn, nt, wt)
 
 
+def combine(FS, TP, W, ht, wdt, out, hs, part, prec, zs, zr, outt, turned, loc, xd_s, xd_r, xo_s, xo_r, cc_s, cc_r, z_s, z_r, fin_s, fin_r):
+    Z = FS // 2
+    H = Z // 2
+    x, f = lax.axis_index("tp"), lax.axis_index("fs")
+    z, c = f // 2, f % 2
+    other = f + 1 - 2 * c
+    ff, block = hs.shape[2], hs.shape[3]
+    half = ff // 2
+    keep = part.shape[1] // 2
+    xside = ((x + 1) % TP, (x + TP - 1) % TP)
+    zside = (((z + 1) % Z) * 2 + c, ((z + Z - 1) % Z) * 2 + c)
+
+    barrier = pltpu.get_barrier_semaphore()
+    for k in xside:
+        pl.semaphore_signal(barrier, inc=1, device_id={"tp": k}, device_id_type=MESH)
+    for k in zside + (other,):
+        pl.semaphore_signal(barrier, inc=1, device_id={"fs": k}, device_id_type=MESH)
+    pl.semaphore_wait(barrier, 5)
+
+    def away(i):
+        return H - (i + 1) // 2
+
+    def chip(i):
+        return jnp.where(i % 2 == 0, (z + away(i)) % Z, (z + Z - away(i)) % Z)
+
+    def mine(i):
+        return ht.at[:, pl.ds(pl.multiple_of(chip(i) * block, LANES), block)]
+
+    def keep_own(i):
+        return pltpu.make_async_copy(mine(i), hs.at[i, x], loc.at[i])
+
+    def direct(i, side):
+        return remote(mine(i), hs.at[i, x], xd_s.at[side, i], xd_r.at[side, i], tp=xside[side])
+
+    def onward(i, side):
+        held = hs.at[i, xside[1 - side], pl.ds(side * half, half)]
+        return remote(held, held, xo_s.at[side, i], xo_r.at[side, i], tp=xside[side])
+
+    def cross(j):
+        return remote(part.at[j, pl.ds((1 - c) * keep, keep)], prec.at[j], cc_s.at[j], cc_r.at[j], fs=other)
+
+    def walk(m, side):
+        k = away(m) - 1
+        return remote(zs.at[m], zr.at[side, k], z_s.at[m], z_r.at[side, k], fs=zside[side])
+
+    def arrival(side, k):
+        return remote(zs.at[0], zr.at[side, k], z_s.at[0], z_r.at[side, k], fs=zside[side])
+
+    def own_first(i, _):
+        keep_own(i).start()
+        return 0
+
+    lax.fori_loop(0, Z, own_first, 0)
+    for i in range(W):
+        for side in (0, 1):
+            direct(i, side).start()
+
+    def step(i, _):
+        @pl.when(i + W < Z)
+        def _():
+            for side in (0, 1):
+                direct(i + W, side).start()
+
+        @pl.when(i < Z)
+        def _():
+            for side in (0, 1):
+                direct(i, side).wait_recv()
+                onward(i, side).start()
+
+        @pl.when((i >= 1) & (i <= Z))
+        def _():
+            j = i - 1
+            keep_own(j).wait()
+            for side in (0, 1):
+                onward(j, side).wait_recv()
+            rhs = hs[j].reshape(TP * ff, block)
+            part[j] = jnp.dot(wdt[...], rhs, preferred_element_type=jnp.float32)
+            cross(j).start()
+
+        @pl.when(i >= 2)
+        def _():
+            m = i - 2
+            k = away(m)
+            cross(m).wait_recv()
+            total = part[m, pl.ds(c * keep, keep)] + prec[m]
+
+            @pl.when(m == 0)
+            def _():
+                zs[m] = total.astype(jnp.bfloat16)
+
+            @pl.when(m == 1)
+            def _():
+                zs[m] = total.astype(jnp.bfloat16)
+
+            for side in (0, 1):
+                @pl.when((m >= 2) & (m < Z - 1) & (m % 2 == side))
+                def _():
+                    arrival(side, k).wait_recv()
+                    zs[m] = (total + zr[side, k].astype(jnp.float32)).astype(jnp.bfloat16)
+
+                @pl.when((m < Z - 1) & (m % 2 == side))
+                def _():
+                    walk(m, side).start()
+
+            @pl.when(m == Z - 1)
+            def _():
+                arrival(0, 0).wait_recv()
+                arrival(1, 0).wait_recv()
+                both = zr[0, 0].astype(jnp.float32) + zr[1, 0].astype(jnp.float32)
+                outt[pl.ds(c * keep, keep)] = (total + both).astype(jnp.bfloat16)
+
+        return 0
+
+    lax.fori_loop(0, Z + 2, step, 0)
+    last = remote(outt.at[pl.ds(c * keep, keep)], outt.at[pl.ds(c * keep, keep)], fin_s, fin_r, fs=other)
+    last.start()
+
+    def drain(i, _):
+        for side in (0, 1):
+            direct(i, side).wait_send()
+            onward(i, side).wait_send()
+        cross(i).wait_send()
+
+        @pl.when(i < Z - 1)
+        def _():
+            arrival_of = remote(zs.at[i], zr.at[0, 0], z_s.at[i], z_r.at[0, 0], fs=other)
+            arrival_of.wait_send()
+
+        return 0
+
+    lax.fori_loop(0, Z, drain, 0)
+    last.wait()
+    turned[...] = outt[...].astype(jnp.float32).T
+    rows = block // 2
+    out[...] = turned[pl.ds(c * rows, rows)].astype(jnp.bfloat16)
+
+
+def run_combine(FS, TP, ht, wdt):
+    Z = FS // 2
+    ff, tokens = ht.shape
+    block = tokens // Z
+    feats = wdt.shape[0]
+    vmem = pl.BlockSpec(memory_space=pltpu.VMEM)
+    return pl.pallas_call(
+        functools.partial(combine, FS, TP, 3),
+        out_shape=jax.ShapeDtypeStruct((block // 2, feats), jnp.bfloat16),
+        in_specs=[vmem] * 2,
+        out_specs=vmem,
+        scratch_shapes=[
+            pltpu.VMEM((Z, TP, ff, block), jnp.bfloat16),
+            pltpu.VMEM((Z, feats, block), jnp.float32),
+            pltpu.VMEM((Z, feats // 2, block), jnp.float32),
+            pltpu.VMEM((Z - 1, feats // 2, block), jnp.bfloat16),
+            pltpu.VMEM((2, Z // 2, feats // 2, block), jnp.bfloat16),
+            pltpu.VMEM((feats, block), jnp.bfloat16),
+            pltpu.VMEM((block, feats), jnp.float32),
+            DMA((Z,)), DMA((2, Z)), DMA((2, Z)), DMA((2, Z)), DMA((2, Z)),
+            DMA((Z,)), DMA((Z,)), DMA((Z - 1,)), DMA((2, Z // 2)), DMA, DMA,
+        ],
+        compiler_params=pltpu.CompilerParams(collective_id=1, has_side_effects=True, vmem_limit_bytes=32 << 20),
+        cost_estimate=pl.CostEstimate(flops=10**9, bytes_accessed=30 << 20, transcendentals=0),
+        name="combine",
+    )(ht, wdt)
+
+
 def body(FS, TP, tokens, routes, route_logits, gain, w_gate, w_up, w_down):
     p = lax.axis_index("grp") % 2
     e = lax.axis_index("tp")
@@ -309,11 +474,9 @@
     gate_act = lax.dot_general(gate_served[0], x_all, contract, preferred_element_type=jnp.float32)
     up_act = lax.dot_general(up_served[0], x_all, contract, preferred_element_type=jnp.float32)
     hidden = (jax.nn.silu(gate_act) * up_act * w_all[None, :].astype(jnp.float32)).astype(jnp.bfloat16)
-    every = lax.all_gather(hidden, "tp", axis=0, tiled=True)
-    down = w_down.astype(jnp.bfloat16).reshape(-1, w_down.shape[2])
-    part = lax.dot_general(every, down, (((0,), (0,)), ((), ())), preferred_element_type=jnp.float32)
-    mixed = lax.psum_scatter(part, "fs", scatter_dimension=0, tiled=True)
-    return (gate_served, up_served, down_served, mixed.astype(jnp.bfloat16))
+    wdt = w_down.astype(jnp.bfloat16).reshape(-1, w_down.shape[2]).T
+    mixed = run_combine(FS, TP, hidden, wdt)
+    return (gate_served, up_served, down_served, mixed)
 
 
 def solution(mesh):

time: 321 us -> 199 us (0.62)
  waiting for transfers between devices: 152 us -> 0 us
  Pallas kernels: 120 us -> 173 us
  between operations: 14.3 us -> 0.86 us
  matrix products: 16.7 us -> 11.2 us
    reduce_scatter x1 -> x0, waiting for transfers between devices: 109 us -> none  [body(): mixed = lax.psum_scatter(part, 'fs', scatter_dimension=0, tiled=True)]
    pallas_call x0 -> x1, Pallas kernels: none -> 53.2 us  [run_combine(): pl.pallas_call(functools.partial(combine, FS, TP, 3), out_shape=jax.Shape...]
    all_gather x1 -> x0, waiting for transfers between devices: 42.6 us -> none  [body(): every = lax.all_gather(hidden, 'tp', axis=0, tiled=True)]
    dot_general x1 -> x0, matrix products: 6.6 us -> none  [body(): lax.dot_general(every, down, (((0,), (0,)), ((), ())), preferred_element_...]
    unnamed x13 -> x20, local copies, waits for them, and re-layouts: 6.69 us -> 5.16 us
  transfers between devices with their start and end apart: 2 -> 0, of which waited for: 2 -> 0; matrix products, arithmetic and copies ran while one was open for 2% -> 0% of each run, Pallas kernels for 0% -> 0%
where the time goes in v2:
time: 199 us
  Pallas kernels  173 us (87%)
  matrix products  11.2 us (6%)
  local copies, waits for them, and re-layouts  10.8 us (5%)
  other arithmetic  3.19 us (2%)
    pallas_call x1, Pallas kernels, run_hand_over(): pl.pallas_call(functools.partial(hand_over, FS, TP), out_shape=(jax.Shape...  120 us
    pallas_call x1, Pallas kernels, run_combine(): pl.pallas_call(functools.partial(combine, FS, TP, 3), out_shape=jax.Shape...  53.2 us
    dot_general x1, matrix products, body(): lax.dot_general(up_served[0], x_all, contract, preferred_element_type=jnp...  6.97 us
    unnamed x20, local copies, waits for them, and re-layouts  5.16 us
    dot_general x1, matrix products, body(): lax.dot_general(gate_served[0], x_all, contract, preferred_element_type=j...  4.25 us

profile of v2, /device:TPU:33, one launch (start us, length us, event | category | flops | bytes accessed | tf_op | source)
XLA Modules:
  0.0 199.1 jit_solution(10487942389990669281)
XLA Ops:
  0.6 0.7 dynamic_slice.14
  1.4 1.6 multiply_convert_fusion.1
  3.0 0.8 reshape.56
  3.8 0.8 reshape.57
  4.6 0.3 copy_bitcast_fusion
  4.8 0.0 copy-start.6
  4.8 0.0 copy-start.7
  4.9 0.0 copy-start.5
  4.9 0.2 pad_maximum_fusion.wp
  5.1 1.2 dynamic-slice_convert_fusion.dn
  6.3 0.0 copy-done.6
  6.3 0.0 copy-done.7
  6.4 0.0 copy-done.5
  6.4 0.2 fusion.2
  6.5 0.1 fusion.3.nt
  6.7 119.9 %hand_over.1 = (bf16[2,32,2,32,224]{4,3,2,1,0:T(8,128)(2,1)S(1)}, bf16[2,112,2048]{2,1,0:T(8,128)(2,1)S(1)}, bf16[32,64,2048]{2,1,0:T(8,128)(2,1)S(1)}, bf16[32,16,128]{2,1,0:T(8,128)(2,1)S(1)}) custom-call(bf16[4,8,2,32,224]{4,3,2,1,0:T(8,128)(2,1)S(1)} %pad_maximum_fusion.wp, bf16[4,112,512]{2,1,0:T(8,128)(2,1)S(1)} %dynamic-slice_convert_fusion.dn, ...), custom_call_target="tpu_custom_call" | custom-call | flops 1000000000 | bytes 31457280 | tf_op jit(solution)/shard_map/hand_over/pallas_call | solution.py:248
  126.6 0.0 copy-start
  126.6 0.2 fusion.5
  126.8 0.0 copy-start.3
  126.9 4.2 %fusion.6 = f32[224,2048]{1,0:T(8,128)} fusion(bf16[2048,224]{1,0:T(8,128)(2,1)S(1)} %bitcast.28, bf16[2048,2048]{1,0:T(8,128)(2,1)S(1)} %bitcast.24), kind=kOutput, calls=%fused_computation.20 | convolution fusion | flops 1879048192 | bytes 11141120 | tf_op jit(solution)/shard_map/dot_general | solution.py:474
  131.2 0.1 reshape.65
  131.2 0.0 copy-done.1
  131.2 7.0 %fusion.1.ht = bf16[224,2048]{1,0:T(8,128)(2,1)S(1)} fusion(bf16[2048,224]{1,0:T(8,128)(2,1)S(1)} %bitcast.26, bf16[2048,2048]{1,0:T(8,128)(2,1)} %bitcast.25, f32[224,2048]{1,0:T(8,128)} %fusion.6, f32[2048]{0:T(1024)S(1)} %reshape.65), kind=kOutput, calls=%fused_computation.2 | convolution fusion | flops 1882259456 | bytes 12066816 | tf_op jit(solution)/shard_map/dot_general | solution.py:475
  138.2 0.0 copy-done.4
  138.2 1.0 convert_element_type.48
  139.3 1.5 copy.16
  140.8 53.2 %combine.1 = bf16[64,512]{1,0:T(8,128)(2,1)S(1)} custom-call(bf16[224,2048]{1,0:T(8,128)(2,1)S(1)} %fusion.1.ht, bf16[512,896]{1,0:T(8,128)(2,1)S(1)} %bitcast.23), custom_call_target="tpu_custom_call" | custom-call | flops 1000000000 | bytes 31457280 | tf_op jit(solution)/shard_map/combine/pallas_call | solution.py:417
  194.0 2.3 %copy.17 = bf16[1,2048,224]{1,2,0:T(8,128)(2,1)} copy(bf16[1,2048,224]{2,1,0:T(8,128)(2,1)} %bitcast.29) | data formatting | bytes 1835008
  196.3 0.0 copy-done.2
  196.3 1.3 copy.18
  197.6 0.9 copy.23
  198.5 0.6 copy.24
  (10 shorter events, 0.1 us)
Async XLA Ops:
  4.8 1.5 copy-start.6
  4.8 1.5 copy-start.7
  4.9 1.5 copy-start.5
  126.6 4.5 %copy-start = (bf16[32,64,2048]{2,1,0:T(8,128)(2,1)}, bf16[32,64,2048]{2,1,0:T(8,128)(2,1)S(1)}, u32[]{:S(2)}) copy-start(bf16[32,64,2048]{2,1,0:T(8,128)(2,1)S(1)} %get-tuple-element.10) | copy-start | bytes 25165828
  126.8 4.3 %copy-start.3 = (bf16[1,32,2,32,224]{4,3,2,1,0:T(8,128)(2,1)}, bf16[1,32,2,32,224]{4,3,2,1,0:T(8,128)(2,1)S(1)}, u32[]{:S(2)}) copy-start(bf16[1,32,2,32,224]{4,3,2,1,0:T(8,128)(2,1)S(1)} %get-tuple-element.21) | copy-start | bytes 2752516
  126.9 4.4 %copy-start.1 = (bf16[1,32,2,32,224]{4,3,2,1,0:T(8,128)(2,1)}, bf16[1,32,2,32,224]{4,3,2,1,0:T(8,128)(2,1)S(1)}, u32[]{:S(2)}) copy-start(bf16[1,32,2,32,224]{4,3,2,1,0:T(8,128)(2,1)S(1)} %get-tuple-element.20) | copy-start | bytes 2752516
  131.2 7.0 %copy-start.4 = (f32[4,224,512]{2,1,0:T(8,128)S(1)}, f32[4,224,512]{2,1,0:T(8,128)}, u32[]{:S(2)}) copy-start(f32[4,224,512]{2,1,0:T(8,128)} %param.13) | copy-start | bytes 5505028
  194.0 2.3 %copy-start.2 = (bf16[1,32,2,32,224]{4,3,2,1,0:T(8,128)(2,1)S(1)}, bf16[1,32,2,32,224]{4,3,2,1,0:T(8,128)(2,1)}, u32[]{:S(2)}) copy-start(bf16[1,32,2,32,224]{4,3,2,1,0:T(8,128)(2,1)} %copy-done.1) | copy-start | bytes 2752516

commit v3 on v2

--- a/solution.py
+++ b/solution.py
@@ -19,20 +19,28 @@
 
 
 def hand_over(
-    FS, TP, wp, dn, nt, wt, gu, ds, tok, wall, xr,
-    xw_s, xw_r, xd_s, xd_r, loc, wt_s, wt_r, rs, rr, xt_s, xt_r, xo_s, xo_r,
+    FS, TP, START, wp, dn, nt, wt, gu, ds, tok, wall, xr, stage,
+    xw_s, xw_r, st_s, st_r, sf_s, sf_r, xd_s, xd_r, loc, wt_s, wt_r, rs, rr, xt_s, xt_r, xo_s, xo_r,
     cc_s, cc_r, za_s, za_r, y_s, y_r, yd_s, yd_r,
 ):
     Z = FS // 2
     H = Z // 2
+    N = H - START + 1
+    B = (Z - 1) // N
+    assert B * N == Z - 1
     x, f, g = lax.axis_index("tp"), lax.axis_index("fs"), lax.axis_index("grp")
     z, c = f // 2, f % 2
     p = g % 2
     mate = g + 1 - 2 * p
     slices = wp.shape[1]
+    hs = slices // 2
     fb = nt.shape[1] // TP
     half = nt.shape[0] // 2
     db = dn.shape[2]
+    other = f + 1 - 2 * c
+    xside = ((x + 1) % TP, (x + TP - 1) % TP)
+    zside = (((z + 1) % Z) * 2 + c, ((z + Z - 1) % Z) * 2 + c)
+    opposite = (x + 2) % TP
 
     def cols(i):
         return pl.ds(pl.multiple_of(i * fb, LANES), fb)
@@ -53,29 +61,50 @@
     pl.semaphore_wait(barrier, FS - 1 + TP - 1 + 1)
 
     def ring(i, fo, side):
-        to = ((z + 1) % Z if side == 0 else (z + Z - 1) % Z) * 2 + c
-        return remote(tok.at[fo, :, cols(x)], tok.at[fo, :, cols(x)], rs.at[side, i], rr.at[side, i], fs=to)
+        return remote(tok.at[fo, :, cols(x)], tok.at[fo, :, cols(x)], rs.at[side, i], rr.at[side, i], fs=zside[side])
 
     def ring_first(side):
-        to = ((z + 1) % Z if side == 0 else (z + Z - 1) % Z) * 2 + c
-        return remote(nt.at[:, cols(x)], tok.at[f, :, cols(x)], rs.at[side, 0], rr.at[side, 0], fs=to)
+        return remote(nt.at[:, cols(x)], tok.at[f, :, cols(x)], rs.at[side, 0], rr.at[side, 0], fs=zside[side])
 
     ring_first(0).start()
     ring_first(1).start()
-    other = f + 1 - 2 * c
+
+    def first_leg(side):
+        return remote(
+            wp.at[opposite, pl.ds(side * hs, hs)], stage.at[side], st_s.at[side], st_r.at[side], tp=xside[side]
+        )
+
+    def second_leg(side):
+        held = xside[1 - side]
+        return remote(
+            stage.at[side], xr.at[held, pl.ds(side * hs, hs)], sf_s.at[side], sf_r.at[side], tp=xside[side]
+        )
+
+    def second_leg_recv(side):
+        return remote(
+            stage.at[side], xr.at[opposite, pl.ds(side * hs, hs)], sf_s.at[side], sf_r.at[side], tp=xside[side]
+        )
+
+    def xw(side):
+        return remote(wp.at[xside[side]], xr.at[x], xw_s.at[side], xw_r.at[side], tp=xside[side])
+
+    def xw_recv(side):
+        return remote(wp.at[x], xr.at[xside[1 - side]], xw_s.at[side], xw_r.at[side], tp=xside[side])
+
+    def xd(k):
+        return remote(dn.at[(x + k) % TP], ds.at[p, :, dcols(x)], xd_s.at[k - 1], xd_r.at[k - 1], tp=(x + k) % TP)
+
+    def xd_recv(k):
+        return remote(
+            dn.at[x], ds.at[p, :, dcols((x + TP - k) % TP)], xd_s.at[k - 1], xd_r.at[k - 1], tp=(x + k) % TP
+        )
+
+    for side in (0, 1):
+        first_leg(side).start()
+    for side in (0, 1):
+        xw(side).start()
     own_cross = remote(nt, tok.at[f], cc_s.at[Z - 1], cc_r.at[Z - 1], fs=other)
     own_cross.start()
-
-    def xw(k):
-        return remote(wp.at[(x + k) % TP], xr.at[x], xw_s.at[k - 1], xw_r.at[k - 1], tp=(x + k) % TP)
-
-    def xd(k):
-        return remote(dn.at[(x + k) % TP], ds.at[p, :, dcols(x)], xd_s.at[k - 1], xd_r.at[k - 1], tp=(x + k) % TP)
-
-    for k in (2, 1, 3):
-        xw(k).start()
-    for k in (2, 1, 3):
-        xd(k).start()
     local = [
         pltpu.make_async_copy(wp.at[x], xr.at[x], loc.at[0]),
         pltpu.make_async_copy(dn.at[x], ds.at[p, :, dcols(x)], loc.at[1]),
@@ -92,8 +121,13 @@
     lax.fori_loop(1, FS, tell, 0)
 
     def across(i, fo, side):
-        to = (x + 1) % TP if side == 0 else (x + TP - 1) % TP
-        return remote(tok.at[fo, :, cols(x)], tok.at[fo, :, cols(x)], xt_s.at[side, i], xt_r.at[side, i], tp=to)
+        return remote(
+            tok.at[fo, :, cols(x)], tok.at[fo, :, cols(x)], xt_s.at[side, i], xt_r.at[side, i], tp=xside[side]
+        )
+
+    def across_recv(i, fo, side):
+        held = tok.at[fo, :, cols(xside[1 - side])]
+        return remote(held, held, xt_s.at[side, i], xt_r.at[side, i], tp=xside[side])
 
     def from_left(s):
         return ((z + Z - s) % Z) * 2 + c
@@ -101,32 +135,49 @@
     def from_right(s):
         return ((z + s) % Z) * 2 + c
 
-    def ring_step(s, _):
+    def origin(i):
+        s = i // 2 + 1
+        return jnp.where(i % 2 == 0, from_left(s), from_right(s))
+
+    def ring_step(s):
         fo = from_left(s)
         ring(s - 1, fo, 0).wait_recv()
-        ring(s, fo, 0).start()
-        fo2 = from_right(s)
-        ring(s - 1, fo2, 1).wait_recv()
-
-        @pl.when(s < H - 1)
-        def _():
-            ring(s, fo2, 1).start()
+
+        @pl.when(s < H)
+        def _():
+            ring(s, fo, 0).start()
 
         for side in (0, 1):
             across(2 * s - 2, fo, side).start()
-            across(2 * s - 1, fo2, side).start()
-        return 0
-
-    lax.fori_loop(1, H, ring_step, 0)
-    last = from_left(H)
-    ring(H - 1, last, 0).wait_recv()
+
+        @pl.when(s < H)
+        def _():
+            fo2 = from_right(s)
+            ring(s - 1, fo2, 1).wait_recv()
+
+            @pl.when(s < H - 1)
+            def _():
+                ring(s, fo2, 1).start()
+
+            for side in (0, 1):
+                across(2 * s - 1, fo2, side).start()
+
+    ring_step(1)
     for side in (0, 1):
-        across(2 * H - 2, last, side).start()
-
-    for copy in local:
-        copy.wait()
+        first_leg(side).wait_recv()
+        second_leg(side).start()
     for k in (2, 1, 3):
-        xw(k).wait_recv()
+        xd(k).start()
+
+    def early(s, _):
+        ring_step(s)
+        return 0
+
+    lax.fori_loop(2, START, early, 0)
+    local[0].wait()
+    for side in (0, 1):
+        xw_recv(side).wait_recv()
+        second_leg_recv(side).wait_recv()
 
     def apart(i):
         m = H - 1 - (i - 1) // 2
@@ -134,86 +185,101 @@
 
     def za(d, cd):
         to = ((z + d) % Z) * 2 + cd
-        return remote(
-            xr.at[to // slices, to % slices], gu.at[:, f, p], za_s.at[d, cd], za_r.at[d, c], fs=to
-        )
+        return remote(xr.at[to // slices, to % slices], gu.at[:, f, p], za_s.at[d, cd], za_r.at[d, c], fs=to)
 
     def za_recv(d, cs):
         fo = ((z + Z - d) % Z) * 2 + cs
         return remote(xr.at[0, 0], gu.at[:, fo, p], za_s.at[d, cs], za_r.at[d, cs], fs=other)
-
-    def za_start(i, _):
-        d = apart(i)
-        za(d, 0).start()
-        za(d, 1).start()
-        return 0
-
-    lax.fori_loop(0, Z - 1, za_start, 0)
-    za(0, 1 - c).start()
-    own = pltpu.make_async_copy(xr.at[f // slices, f % slices], gu.at[:, f, p], loc.at[4])
-    own.start()
-
-    for k in (2, 1, 3):
-        xd(k).wait_recv()
-    yd = remote(ds.at[p], ds.at[p], yd_s, yd_r, grp=mate)
-    yd.start()
 
     def y_hand(d):
         zo = (z + Z - d) % Z
         part = gu.at[:, pl.ds(2 * zo, 2), p]
         return remote(part, part, y_s.at[d], y_r.at[d], grp=mate)
 
-    def origin(i):
-        s = i // 2 + 1
-        return jnp.where(i % 2 == 0, from_left(s), from_right(s))
+    def y_recv(d):
+        zo = (z + Z - d) % Z
+        part = gu.at[:, pl.ds(2 * zo, 2), 1 - p]
+        return remote(part, part, y_s.at[d], y_r.at[d], grp=mate)
 
     def onward(i, fo, side):
-        to = (x + 1) % TP if side == 0 else (x + TP - 1) % TP
-        held = (x + TP - 1) % TP if side == 0 else (x + 1) % TP
-        part = tok.at[fo, pl.ds(side * half, half), cols(held)]
-        return remote(part, part, xo_s.at[side, i], xo_r.at[side, i], tp=to)
+        part = tok.at[fo, pl.ds(side * half, half), cols(xside[1 - side])]
+        return remote(part, part, xo_s.at[side, i], xo_r.at[side, i], tp=xside[side])
+
+    def onward_recv(i, fo, side):
+        part = tok.at[fo, pl.ds(side * half, half), cols(opposite)]
+        return remote(part, part, xo_s.at[side, i], xo_r.at[side, i], tp=xside[side])
 
     def cross(i, fo):
         return remote(tok.at[fo], tok.at[fo], cc_s.at[i], cc_r.at[i], fs=other)
 
-    def finish(i):
-        fo = origin(i)
-        for side in (0, 1):
-            onward(i, fo, side).wait_recv()
-        cross(i, fo).start()
-
-    def flow(i, _):
-        fo = origin(i)
-        for side in (0, 1):
-            across(i, fo, side).wait_recv()
-            onward(i, fo, side).start()
-        d = apart(i)
-        za_recv(d, 0).wait_recv()
-        za_recv(d, 1).wait_recv()
-        y_hand(d).start()
-
-        @pl.when(i > 0)
-        def _():
-            finish(i - 1)
-
-        return 0
-
-    lax.fori_loop(0, Z - 1, flow, 0)
+    def cross_recv(i, fo):
+        return remote(tok.at[fo + 1 - 2 * c], tok.at[fo + 1 - 2 * c], cc_s.at[i], cc_r.at[i], fs=other)
+
+    own = pltpu.make_async_copy(xr.at[f // slices, f % slices], gu.at[:, f, p], loc.at[4])
+    own.start()
+    yd = remote(ds.at[p], ds.at[p], yd_s, yd_r, grp=mate)
+
+    def taken(t):
+        for n in range(B):
+            i = t * B + n
+            fo = origin(i)
+            for side in (0, 1):
+                onward_recv(i, fo, side).wait_recv()
+            cross(i, fo).start()
+        for n in range(B):
+            d = apart(t * B + n)
+            za_recv(d, 0).wait_recv()
+            za_recv(d, 1).wait_recv()
+            y_hand(d).start()
+
+    def flow(t, _):
+        ring_step(START + t)
+        for n in range(B):
+            d = apart(t * B + n)
+            za(d, 0).start()
+            za(d, 1).start()
+        for n in range(B):
+            i = t * B + n
+            fo = origin(i)
+            for side in (0, 1):
+                across_recv(i, fo, side).wait_recv()
+                onward(i, fo, side).start()
+
+        @pl.when(t == 0)
+        def _():
+            za(0, 1 - c).start()
+            local[1].wait()
+            for k in (2, 1, 3):
+                xd_recv(k).wait_recv()
+            yd.start()
+
+        @pl.when(t > 0)
+        def _():
+            taken(t - 1)
+
+        return 0
+
+    lax.fori_loop(0, N, flow, 0)
     own.wait()
     za_recv(0, 1 - c).wait_recv()
     y_hand(0).start()
-    finish(Z - 2)
+    taken(N - 1)
+
+    own_fo = f + 1 - 2 * c
+    remote(nt, tok.at[own_fo], cc_s.at[Z - 1], cc_r.at[Z - 1], fs=other).wait_recv()
 
     def drain(i, _):
         fo = origin(i)
         for side in (0, 1):
             across(i, fo, side).wait_send()
             onward(i, fo, side).wait_send()
-        cross(i, fo).wait()
+        cross(i, fo).wait_send()
+        cross_recv(i, fo).wait_recv()
         d = apart(i)
         za(d, 0).wait_send()
         za(d, 1).wait_send()
-        y_hand(d).wait()
+        y_hand(d).wait_send()
+        y_recv(d).wait_recv()
         return 0
 
     lax.fori_loop(0, Z - 1, drain, 0)
@@ -228,13 +294,20 @@
         return 0
 
     lax.fori_loop(0, H, ring_drain, 0)
-    own_cross.wait()
+    own_cross.wait_send()
     za(0, 1 - c).wait_send()
-    y_hand(0).wait()
-    yd.wait()
-    for k in (1, 2, 3):
-        xw(k).wait_send()
+    y_hand(0).wait_send()
+    y_recv(0).wait_recv()
+    yd.wait_send()
+    remote(ds.at[1 - p], ds.at[1 - p], yd_s, yd_r, grp=mate).wait_recv()
+    for side in (0, 1):
+        first_leg(side).wait_send()
+        second_leg(side).wait_send()
+        xw(side).wait_send()
+    for k in range(1, TP):
         xd(k).wait_send()
+    local[2].wait()
+    local[3].wait()
     tiles = remote(wall.at[pl.ds(0, FS - 1)], wall.at[pl.ds(0, FS - 1)], wt_s, wt_r, fs=other)
     tiles.wait_send()
     tiles.wait_recv()
@@ -244,9 +317,8 @@
     Z = FS // 2
     _, slices, two, half, ff = wp.shape
     vmem = pl.BlockSpec(memory_space=pltpu.VMEM)
-    hbm = pl.BlockSpec(memory_space=pl.ANY)
     return pl.pallas_call(
-        functools.partial(hand_over, FS, TP),
+        functools.partial(hand_over, FS, TP, Z // 4),
         out_shape=(
             jax.ShapeDtypeStruct((two, FS, 2, half, ff), jnp.bfloat16),
             jax.ShapeDtypeStruct((2, dn.shape[1], TP * dn.shape[2]), jnp.bfloat16),
@@ -254,10 +326,12 @@
             jax.ShapeDtypeStruct((FS,) + wt.shape, jnp.bfloat16),
         ),
         in_specs=[vmem] * 4,
-        out_specs=(hbm, hbm, hbm, vmem),
+        out_specs=(vmem,) * 4,
         scratch_shapes=[
             pltpu.VMEM(wp.shape, jnp.bfloat16),
-            DMA((TP - 1,)), DMA((TP - 1,)), DMA((TP - 1,)), DMA((TP - 1,)),
+            pltpu.VMEM((2, slices // 2) + wp.shape[2:], jnp.bfloat16),
+            DMA((2,)), DMA((2,)), DMA((2,)), DMA((2,)), DMA((2,)), DMA((2,)),
+            DMA((TP - 1,)), DMA((TP - 1,)),
             DMA((5,)), DMA, DMA,
             DMA((2, Z // 2)), DMA((2, Z // 2)),
             DMA((2, Z - 1)), DMA((2, Z - 1)), DMA((2, Z - 1)), DMA((2, Z - 1)),
@@ -265,13 +339,52 @@
             DMA((Z, 2)), DMA((Z, 2)),
             DMA((Z,)), DMA((Z,)), DMA, DMA,
         ],
-        compiler_params=pltpu.CompilerParams(collective_id=0, has_side_effects=True, vmem_limit_bytes=32 << 20),
+        compiler_params=pltpu.CompilerParams(collective_id=0, has_side_effects=True, vmem_limit_bytes=8 << 20),
         cost_estimate=pl.CostEstimate(flops=10**9, bytes_accessed=30 << 20, transcendentals=0),
         name="hand_over",
     )(wp, dn, nt, wt)
 
 
-def combine(FS, TP, W, ht, wdt, out, hs, part, prec, zs, zr, outt, turned, loc, xd_s, xd_r, xo_s, xo_r, cc_s, cc_r, z_s, z_r, fin_s, fin_r):
+def expert(block, gu, x, w, ht, gate_out, up_out):
+    features = x.shape[2]
+    count = block // x.shape[1]
+
+    def step(i, _):
+        span = pl.ds(pl.multiple_of(i * block, block), block)
+        part = pl.ds(i * count, count)
+        rows = x[part].reshape(block, features)
+        gate = jnp.dot(rows, gu[0].reshape(features, -1), preferred_element_type=jnp.float32)
+        up = jnp.dot(rows, gu[1].reshape(features, -1), preferred_element_type=jnp.float32)
+        scale = jnp.concatenate([w[i * count + n, 0:1, : x.shape[1]] for n in range(count)], axis=1)
+        ht[:, span] = ((jax.nn.silu(gate) * up).T * scale.astype(jnp.float32)).astype(jnp.bfloat16)
+        for n, served in ((0, gate_out), (1, up_out)):
+            served[:, span] = gu[n, part].reshape(block, -1).astype(jnp.float32).T.astype(jnp.bfloat16)
+        return 0
+
+    lax.fori_loop(0, features // block, step, 0)
+
+
+def run_expert(gu, x, w):
+    tokens, features = x.shape[0] * x.shape[1], x.shape[2]
+    assert tokens == features
+    ff = gu.shape[-1]
+    vmem = pl.BlockSpec(memory_space=pltpu.VMEM)
+    return pl.pallas_call(
+        functools.partial(expert, 256),
+        out_shape=(
+            jax.ShapeDtypeStruct((ff, tokens), jnp.bfloat16),
+            jax.ShapeDtypeStruct((ff, features), jnp.bfloat16),
+            jax.ShapeDtypeStruct((ff, features), jnp.bfloat16),
+        ),
+        in_specs=[vmem] * 3,
+        out_specs=(vmem,) * 3,
+        compiler_params=pltpu.CompilerParams(vmem_limit_bytes=12 << 20),
+        cost_estimate=pl.CostEstimate(flops=4 * 10**9, bytes_accessed=16 << 20, transcendentals=0),
+        name="expert",
+    )(gu, x, w)
+
+
+def combine(FS, TP, W, ht, wd, out, wdt, hs, part, prec, zs, zr, outt, turned, loc, xd_s, xd_r, xo_s, xo_r, cc_s, cc_r, z_s, z_r, fin_s, fin_r):
     Z = FS // 2
     H = Z // 2
     x, f = lax.axis_index("tp"), lax.axis_index("fs")
@@ -327,6 +440,8 @@
     for i in range(W):
         for side in (0, 1):
             direct(i, side).start()
+    for e in range(TP):
+        wdt[:, e * ff : (e + 1) * ff] = wd[e].T.astype(jnp.bfloat16)
 
     def step(i, _):
         @pl.when(i + W < Z)
@@ -408,11 +523,11 @@
     out[...] = turned[pl.ds(c * rows, rows)].astype(jnp.bfloat16)
 
 
-def run_combine(FS, TP, ht, wdt):
+def run_combine(FS, TP, ht, wd):
     Z = FS // 2
     ff, tokens = ht.shape
     block = tokens // Z
-    feats = wdt.shape[0]
+    feats = wd.shape[2]
     vmem = pl.BlockSpec(memory_space=pltpu.VMEM)
     return pl.pallas_call(
         functools.partial(combine, FS, TP, 3),
@@ -420,6 +535,7 @@
         in_specs=[vmem] * 2,
         out_specs=vmem,
         scratch_shapes=[
+            pltpu.VMEM((feats, TP * ff), jnp.bfloat16),
             pltpu.VMEM((Z, TP, ff, block), jnp.bfloat16),
             pltpu.VMEM((Z, feats, block), jnp.float32),
             pltpu.VMEM((Z, feats // 2, block), jnp.float32),
@@ -430,10 +546,10 @@
             DMA((Z,)), DMA((2, Z)), DMA((2, Z)), DMA((2, Z)), DMA((2, Z)),
             DMA((Z,)), DMA((Z,)), DMA((Z - 1,)), DMA((2, Z // 2)), DMA, DMA,
         ],
-        compiler_params=pltpu.CompilerParams(collective_id=1, has_side_effects=True, vmem_limit_bytes=32 << 20),
+        compiler_params=pltpu.CompilerParams(collective_id=1, has_side_effects=True, vmem_limit_bytes=20 << 20),
         cost_estimate=pl.CostEstimate(flops=10**9, bytes_accessed=30 << 20, transcendentals=0),
         name="combine",
-    )(ht, wdt)
+    )(ht, wd)
 
 
 def body(FS, TP, tokens, routes, route_logits, gain, w_gate, w_up, w_down):
@@ -464,19 +580,9 @@
     wt = jnp.broadcast_to(jnp.pad(weight, (0, LANES - count))[None], (16, LANES))
 
     gu, ds, tok, wall = run_hand_over(FS, TP, wp, dn, nt, wt)
-    gate_served = gu[0].reshape(1, FS * rows, ff // slices)
-    up_served = gu[1].reshape(1, FS * rows, ff // slices)
-    down_served = ds.reshape(1, 2 * hrows, TP * dn.shape[2])
-    x_all = tok.reshape(FS * count, -1)
-    w_all = wall[:, 0, :count].reshape(FS * count)
-
-    contract = (((0,), (1,)), ((), ()))
-    gate_act = lax.dot_general(gate_served[0], x_all, contract, preferred_element_type=jnp.float32)
-    up_act = lax.dot_general(up_served[0], x_all, contract, preferred_element_type=jnp.float32)
-    hidden = (jax.nn.silu(gate_act) * up_act * w_all[None, :].astype(jnp.float32)).astype(jnp.bfloat16)
-    wdt = w_down.astype(jnp.bfloat16).reshape(-1, w_down.shape[2]).T
-    mixed = run_combine(FS, TP, hidden, wdt)
-    return (gate_served, up_served, down_served, mixed)
+    hidden, gate_t, up_t = run_expert(gu, tok, wall)
+    mixed = run_combine(FS, TP, hidden, w_down)
+    return (gate_t.T[None], up_t.T[None], ds.reshape(1, 2 * hrows, -1), mixed)
 
 
 def solution(mesh):

time: 199 us -> 183 us (0.920)
  matrix products: 11.2 us -> 0 us
  local copies, waits for them, and re-layouts: 10.8 us -> 5.34 us
    dot_general x2 -> x0, matrix products: 11.2 us -> none  [the longest x1 6.97 us: body(): lax.dot_general(up_served[0], x_all, contract, preferred_element_type=jnp...]
    pallas_call x1 -> x2, Pallas kernels: 120 us -> 116 us  [the longest x1 109 us: run_hand_over(): pl.pallas_call(functools.partial(hand_over, FS, TP, Z // 4), out_shape=(j...]
    unnamed x20 -> x4, local copies, waits for them, and re-layouts: 5.16 us -> 1.56 us
    pallas_call x1, Pallas kernels: 53.2 us -> 55.7 us  [run_combine(): pl.pallas_call(functools.partial(combine, FS, TP, 3), out_shape=jax.Shape...]
where the time goes in v3:
time: 183 us
  Pallas kernels  172 us (94%)
  local copies, waits for them, and re-layouts  5.34 us (3%)
  other arithmetic  4.76 us (3%)
    pallas_call x1, Pallas kernels, run_hand_over(): pl.pallas_call(functools.partial(hand_over, FS, TP, Z // 4), out_shape=(j...  109 us
    pallas_call x1, Pallas kernels, run_combine(): pl.pallas_call(functools.partial(combine, FS, TP, 3), out_shape=jax.Shape...  55.7 us
    pallas_call x1, Pallas kernels, run_expert(): pl.pallas_call(functools.partial(expert, 256), out_shape=(jax.ShapeDtypeS...  7.63 us

profile of v3, /device:TPU:33, one launch (start us, length us, event | category | flops | bytes accessed | tf_op | source)
XLA Modules:
  0.0 182.8 jit_solution(7390956026439629163)
XLA Ops:
  0.7 0.8 convert_bitcast_fusion
  1.4 0.7 dynamic_slice.14
  2.2 1.1 fusion
  3.3 1.1 fusion.1.nt
  4.4 1.2 dynamic-slice_convert_fusion.dn
  5.6 1.6 multiply_convert_fusion.1
  7.3 0.8 reshape.41
  8.0 0.8 reshape.42
  8.8 0.3 copy_bitcast_fusion
  9.1 0.2 pad_maximum_fusion.wp
  9.3 108.6 %hand_over.1 = (bf16[2,32,2,32,224]{4,3,2,1,0:T(8,128)(2,1)S(1)}, bf16[2,112,2048]{2,1,0:T(8,128)(2,1)S(1)}, bf16[32,64,2048]{2,1,0:T(8,128)(2,1)S(1)}, bf16[32,16,128]{2,1,0:T(8,128)(2,1)S(1)}) custom-call(bf16[4,8,2,32,224]{4,3,2,1,0:T(8,128)(2,1)S(1)} %pad_maximum_fusion.wp, bf16[4,112,512]{2,1,0:T(8,128)(2,1)S(1)} %dynamic-slice_convert_fusion.dn, ...), custom_call_target="tpu_custom_call" | custom-call | flops 1000000000 | bytes 31457280 | tf_op jit(solution)/shard_map/hand_over/pallas_call | solution.py:320
  117.9 0.0 copy-start
  117.9 7.6 %expert.1 = (bf16[224,2048]{1,0:T(8,128)(2,1)S(1)}, bf16[224,2048]{1,0:T(8,128)(2,1)}, bf16[224,2048]{1,0:T(8,128)(2,1)}) custom-call(bf16[2,32,2,32,224]{4,3,2,1,0:T(8,128)(2,1)S(1)} %get-tuple-element.11.gu, bf16[32,64,2048]{2,1,0:T(8,128)(2,1)S(1)} %get-tuple-element.12.x, bf16[32,16,128]{2,1,0:T(8,128)(2,1)S(1)} %get-tuple-element.13.w), custom_call_target="tpu_custom_call" | custom-call | flops 4000000000 | bytes 16777216 | tf_op jit(solution)/shard_map/expert/pallas_call | solution.py:372
  125.6 0.0 copy-done
  125.6 55.7 %combine.1 = bf16[64,512]{1,0:T(8,128)(2,1)S(1)} custom-call(bf16[224,2048]{1,0:T(8,128)(2,1)S(1)} %get-tuple-element.17.ht, f32[4,224,512]{2,1,0:T(8,128)S(1)} %copy-done), custom_call_target="tpu_custom_call" | custom-call | flops 1000000000 | bytes 31457280 | tf_op jit(solution)/shard_map/combine/pallas_call | solution.py:532
  181.2 0.9 copy.17
  182.2 0.6 copy.18
  (3 shorter events, 0.0 us)
Async XLA Ops:
  117.9 7.6 %copy-start = (f32[4,224,512]{2,1,0:T(8,128)S(1)}, f32[4,224,512]{2,1,0:T(8,128)}, u32[]{:S(2)}) copy-start(f32[4,224,512]{2,1,0:T(8,128)} %wd.1) | copy-start | bytes 5505028

commit v4 on v3

v4 whole, which is shorter than its diff:
```python
import functools

import jax
import jax.numpy as jnp
from jax import lax
from jax.experimental import pallas as pl
from jax.experimental.pallas import tpu as pltpu
from jax.sharding import PartitionSpec as P

MESH = pl.DeviceIdType.MESH
DMA = pltpu.SemaphoreType.DMA
LANES = 128


def remote(src, dst, send, recv, **where):
    return pltpu.make_async_remote_copy(
        src_ref=src, dst_ref=dst, send_sem=send, recv_sem=recv, device_id=where, device_id_type=MESH
    )


def hand_over(
    FS, TP, x_in, routes, logits, gain, w_gate, w_up, w_down, gu, ds, tok, wall,
    raw_gate, raw_up, raw_down, scale, wp, dn, nt, wt, xr, stage,
    in_s, loc, xw_s, xw_r, st_s, st_r, sf_s, sf_r, xd_s, xd_r, rs, rr, ws, wr, xt_s, xt_r, xo_s, xo_r,
    cc_s, cc_r, cw_s, cw_r, za_s, za_r, y_s, y_r, yd_s, yd_r,
):
    Z = FS // 2
    H = Z // 2
    Q = Z // TP
    assert TP == 4 and Q * TP == Z and H == 2 * Q
    x, f, g = lax.axis_index("tp"), lax.axis_index("fs"), lax.axis_index("grp")
    z, c = f // 2, f % 2
    zone, seat = z // Q, z % Q
    p = g % 2
    mate = g + 1 - 2 * p
    fb = nt.shape[1] // TP
    half = nt.shape[0] // 2
    db = dn.shape[2]
    rows = raw_gate.shape[1]
    drows = raw_down.shape[1]
    other = f + 1 - 2 * c
    xside = ((x + 1) % TP, (x + TP - 1) % TP)
    zside = (((z + 1) % Z) * 2 + c, ((z + Z - 1) % Z) * 2 + c)
    opposite = (x + 2) % TP

    fetch = (
        pltpu.make_async_copy(w_gate.at[:, pl.ds(p * rows, rows)], raw_gate, in_s.at[0]),
        pltpu.make_async_copy(w_up.at[:, pl.ds(p * rows, rows)], raw_up, in_s.at[1]),
        pltpu.make_async_copy(w_down.at[:, pl.ds(p * drows, drows)], raw_down, in_s.at[2]),
    )
    for copy in fetch:
        copy.start()

    barrier = pltpu.get_barrier_semaphore()

    def greet(r, _):
        pl.semaphore_signal(barrier, inc=1, device_id={"fs": (f + r) % FS}, device_id_type=MESH)
        return 0

    lax.fori_loop(1, FS, greet, 0)
    for k in range(1, TP):
        pl.semaphore_signal(barrier, inc=1, device_id={"tp": (x + k) % TP}, device_id_type=MESH)
    pl.semaphore_signal(barrier, inc=1, device_id={"grp": mate}, device_id_type=MESH)

    values = x_in[...].astype(jnp.float32)
    mean_square = jnp.mean(values * values, axis=-1, keepdims=True)
    nt[...] = (values * lax.rsqrt(mean_square + 1e-06)).astype(jnp.bfloat16)
    count = routes.shape[1]
    first = jax.nn.sigmoid(logits[0:1] - logits[1:2])
    second = jax.nn.sigmoid(logits[1:2] - logits[0:1])
    weight = first * (routes[0:1] == x).astype(jnp.float32) + second * (routes[1:2] == x).astype(jnp.float32)
    wt[...] = jnp.zeros_like(wt)
    wt[:, :count] = jnp.broadcast_to(weight, (wt.shape[0], count)).astype(jnp.bfloat16)
    scale[...] = jnp.broadcast_to(gain[...], (LANES, gain.shape[1])).T
    factor = scale[pl.ds(p * rows, rows), :][:, :1]
    ff = wp.shape[4] // 4
    part = rows // 2
    fetch[0].wait()
    fetch[1].wait()

    def pack(e, _):
        gate = raw_gate[e] * factor
        up = raw_up[e] * factor
        for j in range(2 * Q):
            span = slice(j * ff, (j + 1) * ff)
            quarters = [gate[:part, span], up[:part, span], gate[part:, span], up[part:, span]]
            wp[e, j // 2, j % 2] = jnp.concatenate(quarters, axis=1).astype(jnp.bfloat16)
        return 0

    lax.fori_loop(0, TP, pack, 0)
    fetch[2].wait()
    dn[...] = raw_down[...].astype(jnp.bfloat16)

    pl.semaphore_wait(barrier, FS - 1 + TP - 1 + 1)

    def cols(i):
        return pl.ds(pl.multiple_of(i * fb, LANES), fb)

    def dcols(i):
        return pl.ds(pl.multiple_of(i * db, LANES), db)

    def ring(i, fo, side):
        return remote(tok.at[fo, :, cols(x)], tok.at[fo, :, cols(x)], rs.at[side, i], rr.at[side, i], fs=zside[side])

    def ring_w(i, fo, side):
        return remote(wall.at[fo], wall.at[fo], ws.at[side, i], wr.at[side, i], fs=zside[side])

    for side in (0, 1):
        remote(nt.at[:, cols(x)], tok.at[f, :, cols(x)], rs.at[side, 0], rr.at[side, 0], fs=zside[side]).start()
        remote(wt, wall.at[f], ws.at[side, 0], wr.at[side, 0], fs=zside[side]).start()

    def spot(n):
        return (seat + n) % Q

    def xw(n, side):
        return remote(wp.at[xside[side], spot(n)], xr.at[x, spot(n)], xw_s.at[side, n], xw_r.at[side, n], tp=xside[side])

    def xw_recv(n, side):
        held = xr.at[xside[1 - side], spot(n)]
        return remote(held, held, xw_s.at[side, n], xw_r.at[side, n], tp=xside[side])

    def first_leg(n):
        return remote(wp.at[opposite, spot(n)], stage.at[n], st_s.at[n], st_r.at[n], tp=xside[n % 2])

    def second_leg(n):
        return remote(stage.at[n], xr.at[xside[1 - n % 2], spot(n)], sf_s.at[n], sf_r.at[n], tp=xside[n % 2])

    def second_leg_recv(n):
        return remote(stage.at[n], xr.at[opposite, spot(n)], sf_s.at[n], sf_r.at[n], tp=xside[n % 2])

    def xd(k):
        return remote(dn.at[(x + k) % TP], ds.at[p, :, dcols(x)], xd_s.at[k - 1], xd_r.at[k - 1], tp=(x + k) % TP)

    def xd_recv(k):
        held = ds.at[p, :, dcols((x + TP - k) % TP)]
        return remote(held, held, xd_s.at[k - 1], xd_r.at[k - 1], tp=(x + k) % TP)

    for n in range(Q):
        first_leg(n).start()
        for side in (0, 1):
            xw(n, side).start()
    own_cross = remote(nt, tok.at[f], cc_s.at[Z - 1], cc_r.at[Z - 1], fs=other)
    own_cross.start()
    own_cross_w = remote(wt, wall.at[f], cw_s.at[Z - 1], cw_r.at[Z - 1], fs=other)
    own_cross_w.start()
    local = [
        pltpu.make_async_copy(wp.at[x], xr.at[x], loc.at[0]),
        pltpu.make_async_copy(dn.at[x], ds.at[p, :, dcols(x)], loc.at[1]),
        pltpu.make_async_copy(nt, tok.at[f], loc.at[2]),
        pltpu.make_async_copy(wt, wall.at[f], loc.at[3]),
    ]
    for copy in local:
        copy.start()

    def across(i, fo, side):
        return remote(
            tok.at[fo, :, cols(x)], tok.at[fo, :, cols(x)], xt_s.at[side, i], xt_r.at[side, i], tp=xside[side]
        )

    def across_recv(i, fo, side):
        held = tok.at[fo, :, cols(xside[1 - side])]
        return remote(held, held, xt_s.at[side, i], xt_r.at[side, i], tp=xside[side])

    def from_left(s):
        return ((z + Z - s) % Z) * 2 + c

    def from_right(s):
        return ((z + s) % Z) * 2 + c

    def origin(i):
        s = i // 2 + 1
        return jnp.where(i % 2 == 0, from_left(s), from_right(s))

    def ring_step(s):
        for side in (0, 1):
            if s < H or side == 0:
                fo = from_left(s) if side == 0 else from_right(s)
                ring(s - 1, fo, side).wait_recv()
                ring_w(s - 1, fo, side).wait_recv()
                if s < H - side:
                    ring(s, fo, side).start()
                    ring_w(s, fo, side).start()
                for way in (0, 1):
                    across(2 * s - 2 + side, fo, way).start()

    turns = ((1, 3), (2, 0))

    def za(n, u, cd):
        zc = ((zone + u) % TP) * Q + spot(n)
        return remote(
            xr.at[zc // Q, spot(n), cd], gu.at[f, p], za_s.at[n * TP + u, cd], za_r.at[n * TP + u, c], fs=zc * 2 + cd
        )

    def source(n, u):
        return ((zone + TP - u) % TP) * Q + (seat + Q - n) % Q

    def za_recv(n, u, cs):
        held = gu.at[2 * source(n, u) + cs, p]
        return remote(held, held, za_s.at[n * TP + u, cs], za_r.at[n * TP + u, cs], fs=other)

    def y_hand(n, u):
        held = gu.at[pl.ds(2 * source(n, u), 2), p]
        return remote(held, held, y_s.at[n * TP + u], y_r.at[n * TP + u], grp=mate)

    def y_recv(n, u):
        held = gu.at[pl.ds(2 * source(n, u), 2), 1 - p]
        return remote(held, held, y_s.at[n * TP + u], y_r.at[n * TP + u], grp=mate)

    own = pltpu.make_async_copy(xr.at[zone, seat, c], gu.at[f, p], loc.at[4])

    def issue(b):
        n = b // 2
        if b % 2 == 0:
            for side in (0, 1):
                xw_recv(n, side).wait_recv()
            second_leg_recv(n).wait_recv()
        for u in turns[b % 2]:
            if n == 0 and u == 0:
                za(0, 0, 1 - c).start()
                own.start()
            else:
                za(n, u, 0).start()
                za(n, u, 1).start()

    def accept(b):
        n = b // 2
        for u in turns[b % 2]:
            if n == 0 and u == 0:
                own.wait()
                za_recv(0, 0, 1 - c).wait_recv()
            else:
                za_recv(n, u, 0).wait_recv()
                za_recv(n, u, 1).wait_recv()
            y_hand(n, u).start()

    def onward(i, fo, side):
        held = tok.at[fo, pl.ds(side * half, half), cols(xside[1 - side])]
        return remote(held, held, xo_s.at[side, i], xo_r.at[side, i], tp=xside[side])

    def onward_recv(i, fo, side):
        held = tok.at[fo, pl.ds(side * half, half), cols(opposite)]
        return remote(held, held, xo_s.at[side, i], xo_r.at[side, i], tp=xside[side])

    def cross(i, fo):
        return remote(tok.at[fo], tok.at[fo], cc_s.at[i], cc_r.at[i], fs=other)

    def cross_w(i, fo):
        return remote(wall.at[fo], wall.at[fo], cw_s.at[i], cw_r.at[i], fs=other)

    def cross_recv(i, fo):
        return remote(tok.at[fo + 1 - 2 * c], tok.at[fo + 1 - 2 * c], cc_s.at[i], cc_r.at[i], fs=other)

    def cross_w_recv(i, fo):
        return remote(wall.at[fo + 1 - 2 * c], wall.at[fo + 1 - 2 * c], cw_s.at[i], cw_r.at[i], fs=other)

    def pass_on(i):
        fo = origin(i)
        for side in (0, 1):
            across_recv(i, fo, side).wait_recv()
            onward(i, fo, side).start()

    def finish(i):
        fo = origin(i)
        for side in (0, 1):
            onward_recv(i, fo, side).wait_recv()
        cross(i, fo).start()
        cross_w(i, fo).start()

    yd = remote(ds.at[p], ds.at[p], yd_s, yd_r, grp=mate)
    ring_step(1)
    for n in (0, 1):
        first_leg(n).wait_recv()
        second_leg(n).start()
    for n in range(2, Q):
        first_leg(n).wait_recv()
        second_leg(n).start()
    for k in (2, 1, 3):
        xd(k).start()
    ring_step(2)
    local[0].wait()
    issue(0)
    for s in range(3, H + 1):
        ring_step(s)
        issue(s - 2)
        if s == H:
            issue(s - 1)
        for i in (2 * s - 6, 2 * s - 5):
            pass_on(i)
        if s == 4:
            local[1].wait()
            for k in (2, 1, 3):
                xd_recv(k).wait_recv()
            yd.start()
        if s > 3:
            for i in (2 * s - 8, 2 * s - 7):
                finish(i)
            accept(s - 4)
    pass_on(2 * H - 4)
    pass_on(2 * H - 3)
    finish(2 * H - 6)
    finish(2 * H - 5)
    accept(H - 3)
    pass_on(2 * H - 2)
    finish(2 * H - 4)
    finish(2 * H - 3)
    accept(H - 2)
    finish(2 * H - 2)
    accept(H - 1)

    local[2].wait()
    local[3].wait()
    own_fo = f + 1 - 2 * c
    remote(nt, tok.at[own_fo], cc_s.at[Z - 1], cc_r.at[Z - 1], fs=other).wait_recv()
    remote(wt, wall.at[own_fo], cw_s.at[Z - 1], cw_r.at[Z - 1], fs=other).wait_recv()
    own_cross.wait_send()
    own_cross_w.wait_send()

    def drain(i, _):
        fo = origin(i)
        for side in (0, 1):
            across(i, fo, side).wait_send()
            onward(i, fo, side).wait_send()
        cross(i, fo).wait_send()
        cross_w(i, fo).wait_send()
        cross_recv(i, fo).wait_recv()
        cross_w_recv(i, fo).wait_recv()
        return 0

    lax.fori_loop(0, Z - 1, drain, 0)

    def ring_drain(s, _):
        ring(s, f, 0).wait_send()
        ring_w(s, f, 0).wait_send()

        @pl.when(s < H - 1)
        def _():
            ring(s, f, 1).wait_send()
            ring_w(s, f, 1).wait_send()

        return 0

    lax.fori_loop(0, H, ring_drain, 0)
    za(0, 0, 1 - c).wait_send()
    y_hand(0, 0).wait_send()
    y_recv(0, 0).wait_recv()

    def exchange_drain(v, _):
        n, u = v // TP, v % TP
        za(n, u, 0).wait_send()
        za(n, u, 1).wait_send()
        y_hand(n, u).wait_send()
        y_recv(n, u).wait_recv()
        return 0

    lax.fori_loop(1, Z, exchange_drain, 0)
    yd.wait_send()
    remote(ds.at[1 - p], ds.at[1 - p], yd_s, yd_r, grp=mate).wait_recv()
    for n in range(Q):
        first_leg(n).wait_send()
        second_leg(n).wait_send()
        for side in (0, 1):
            xw(n, side).wait_send()
    for k in range(1, TP):
        xd(k).wait_send()


def run_hand_over(FS, TP, tokens, routes, logits, gain, w_gate, w_up, w_down):
    Z = FS // 2
    Q = Z // TP
    _, rows, ff = w_gate.shape
    ff = ff // (2 * Q)
    half = rows // 2
    drows, db = w_down.shape[1] // 2, w_down.shape[2]
    vmem = pl.BlockSpec(memory_space=pltpu.VMEM)
    hbm = pl.BlockSpec(memory_space=pl.ANY)
    tile = (16, LANES)
    piece = (half // 2, 4 * ff)
    bf16 = jnp.bfloat16
    return pl.pallas_call(
        functools.partial(hand_over, FS, TP),
        out_shape=(
            jax.ShapeDtypeStruct((FS, 2) + piece, bf16),
            jax.ShapeDtypeStruct((2, drows, TP * db), bf16),
            jax.ShapeDtypeStruct((FS,) + tokens.shape, bf16),
            jax.ShapeDtypeStruct((FS,) + tile, bf16),
        ),
        in_specs=[vmem] * 4 + [hbm] * 3,
        out_specs=(vmem,) * 4,
        scratch_shapes=[
            pltpu.VMEM((TP, half, w_gate.shape[2]), jnp.float32),
            pltpu.VMEM((TP, half, w_gate.shape[2]), jnp.float32),
            pltpu.VMEM((TP, drows, db), jnp.float32),
            pltpu.VMEM((rows, LANES), jnp.float32),
            pltpu.VMEM((TP, Q, 2) + piece, bf16),
            pltpu.VMEM((TP, drows, db), bf16),
            pltpu.VMEM(tokens.shape, bf16),
            pltpu.VMEM(tile, bf16),
            pltpu.VMEM((TP, Q, 2) + piece, bf16),
            pltpu.VMEM((Q, 2) + piece, bf16),
            DMA((3,)), DMA((5,)),
            DMA((2, Q)), DMA((2, Q)), DMA((Q,)), DMA((Q,)), DMA((Q,)), DMA((Q,)),
            DMA((TP - 1,)), DMA((TP - 1,)),
            DMA((2, Z // 2)), DMA((2, Z // 2)), DMA((2, Z // 2)), DMA((2, Z // 2)),
            DMA((2, Z - 1)), DMA((2, Z - 1)), DMA((2, Z - 1)), DMA((2, Z - 1)),
            DMA((Z,)), DMA((Z,)), DMA((Z,)), DMA((Z,)),
            DMA((Z, 2)), DMA((Z, 2)),
            DMA((Z,)), DMA((Z,)), DMA, DMA,
        ],
        compiler_params=pltpu.CompilerParams(collective_id=0, has_side_effects=True, vmem_limit_bytes=16 << 20),
        cost_estimate=pl.CostEstimate(flops=10**9, bytes_accessed=30 << 20, transcendentals=0),
        name="hand_over",
    )(tokens, routes, logits, gain, w_gate, w_up, w_down)


def expert(block, gu, x, w, ht, gate_out, up_out, wg, wu):
    features = x.shape[2]
    count = block // x.shape[1]
    part, ff = gu.shape[2], gu.shape[3] // 4
    pieces = block // (2 * part)

    def unpack(i, _):
        span = pl.ds(pl.multiple_of(i * block, block), block)
        for v in range(pieces):
            k = i * pieces + v
            piece = gu[k // 2, k % 2].astype(jnp.float32)
            for hh in (0, 1):
                at = pl.ds(pl.multiple_of(k * 2 * part + hh * part, part), part)
                wg[at, :] = piece[:, 2 * hh * ff : (2 * hh + 1) * ff].astype(jnp.bfloat16)
                wu[at, :] = piece[:, (2 * hh + 1) * ff : (2 * hh + 2) * ff].astype(jnp.bfloat16)
        for own, served in ((wg, gate_out), (wu, up_out)):
            served[:, span] = own[span, :].astype(jnp.float32).T.astype(jnp.bfloat16)
        return 0

    lax.fori_loop(0, features // block, unpack, 0)

    def step(i, _):
        span = pl.ds(pl.multiple_of(i * block, block), block)
        rows = x[pl.ds(i * count, count)].reshape(block, features)
        gate = jnp.dot(rows, wg[...], preferred_element_type=jnp.float32)
        up = jnp.dot(rows, wu[...], preferred_element_type=jnp.float32)
        scale = jnp.concatenate([w[i * count + n, 0:1, : x.shape[1]] for n in range(count)], axis=1)
        ht[:, span] = ((jax.nn.silu(gate) * up).T * scale.astype(jnp.float32)).astype(jnp.bfloat16)
        return 0

    lax.fori_loop(0, x.shape[0] // count, step, 0)


def run_expert(gu, x, w):
    tokens, features = x.shape[0] * x.shape[1], x.shape[2]
    ff = gu.shape[3] // 4
    vmem = pl.BlockSpec(memory_space=pltpu.VMEM)
    bf16 = jnp.bfloat16
    return pl.pallas_call(
        functools.partial(expert, 256),
        out_shape=(
            jax.ShapeDtypeStruct((ff, tokens), bf16),
            jax.ShapeDtypeStruct((ff, features), bf16),
            jax.ShapeDtypeStruct((ff, features), bf16),
        ),
        in_specs=[vmem] * 3,
        out_specs=(vmem,) * 3,
        scratch_shapes=[pltpu.VMEM((features, ff), bf16), pltpu.VMEM((features, ff), bf16)],
        compiler_params=pltpu.CompilerParams(vmem_limit_bytes=12 << 20),
        cost_estimate=pl.CostEstimate(flops=4 * 10**9, bytes_accessed=16 << 20, transcendentals=0),
        name="expert",
    )(gu, x, w)


def combine(FS, TP, W, L, ht, wd, out, wdt, hs, part, prec, zs, zr, outt, turned, loc, xd_s, xd_r, xo_s, xo_r, cc_s, cc_r, z_s, z_r, fin_s, fin_r):
    Z = FS // 2
    H = Z // 2
    x, f = lax.axis_index("tp"), lax.axis_index("fs")
    z, c = f // 2, f % 2
    other = f + 1 - 2 * c
    ff, block = hs.shape[2], hs.shape[3]
    half = ff // 2
    keep = part.shape[1] // 2
    xside = ((x + 1) % TP, (x + TP - 1) % TP)
    zside = (((z + 1) % Z) * 2 + c, ((z + Z - 1) % Z) * 2 + c)

    barrier = pltpu.get_barrier_semaphore()
    for k in xside:
        pl.semaphore_signal(barrier, inc=1, device_id={"tp": k}, device_id_type=MESH)
    for k in zside + (other,):
        pl.semaphore_signal(barrier, inc=1, device_id={"fs": k}, device_id_type=MESH)
    pl.semaphore_wait(barrier, 5)

    def away(i):
        return H - (i + 1) // 2

    def chip(i):
        return jnp.where(i % 2 == 0, (z + away(i)) % Z, (z + Z - away(i)) % Z)

    def mine(i):
        return ht.at[:, pl.ds(pl.multiple_of(chip(i) * block, LANES), block)]

    def keep_own(i):
        return pltpu.make_async_copy(mine(i), hs.at[i, x], loc.at[i])

    def direct(i, side):
        return remote(mine(i), hs.at[i, x], xd_s.at[side, i], xd_r.at[side, i], tp=xside[side])

    def onward(i, side):
        held = hs.at[i, xside[1 - side], pl.ds(side * half, half)]
        return remote(held, held, xo_s.at[side, i], xo_r.at[side, i], tp=xside[side])

    def cross(j):
        return remote(part.at[j, pl.ds((1 - c) * keep, keep)], prec.at[j], cc_s.at[j], cc_r.at[j], fs=other)

    def walk(m, side):
        k = away(m) - 1
        return remote(zs.at[m], zr.at[side, k], z_s.at[m], z_r.at[side, k], fs=zside[side])

    def arrival(side, k):
        return remote(zs.at[0], zr.at[side, k], z_s.at[0], z_r.at[side, k], fs=zside[side])

    def own_first(i, _):
        keep_own(i).start()
        return 0

    lax.fori_loop(0, Z, own_first, 0)
    for i in range(W):
        for side in (0, 1):
            direct(i, side).start()
    for e in range(TP):
        wdt[:, e * ff : (e + 1) * ff] = wd[e].T.astype(jnp.bfloat16)

    def step(i, _):
        @pl.when(i + W < Z)
        def _():
            for side in (0, 1):
                direct(i + W, side).start()

        @pl.when(i < Z)
        def _():
            for side in (0, 1):
                direct(i, side).wait_recv()
                onward(i, side).start()

        @pl.when((i >= L) & (i < Z + L))
        def _():
            j = i - L
            keep_own(j).wait()
            for side in (0, 1):
                onward(j, side).wait_recv()
            rhs = hs[j].reshape(TP * ff, block)
            part[j] = jnp.dot(wdt[...], rhs, preferred_element_type=jnp.float32)
            cross(j).start()

        @pl.when(i > L)
        def _():
            m = i - L - 1
            k = away(m)
            cross(m).wait_recv()
            total = part[m, pl.ds(c * keep, keep)] + prec[m]

            @pl.when(m == 0)
            def _():
                zs[m] = total.astype(jnp.bfloat16)

            @pl.when(m == 1)
            def _():
                zs[m] = total.astype(jnp.bfloat16)

            for side in (0, 1):
                @pl.when((m >= 2) & (m < Z - 1) & (m % 2 == side))
                def _():
                    arrival(side, k).wait_recv()
                    zs[m] = (total + zr[side, k].astype(jnp.float32)).astype(jnp.bfloat16)

                @pl.when((m < Z - 1) & (m % 2 == side))
                def _():
                    walk(m, side).start()

            @pl.when(m == Z - 1)
            def _():
                arrival(0, 0).wait_recv()
                arrival(1, 0).wait_recv()
                both = zr[0, 0].astype(jnp.float32) + zr[1, 0].astype(jnp.float32)
                outt[pl.ds(c * keep, keep)] = (total + both).astype(jnp.bfloat16)

        return 0

    lax.fori_loop(0, Z + L + 1, step, 0)
    last = remote(outt.at[pl.ds(c * keep, keep)], outt.at[pl.ds(c * keep, keep)], fin_s, fin_r, fs=other)
    last.start()

    def drain(i, _):
        for side in (0, 1):
            direct(i, side).wait_send()
            onward(i, side).wait_send()
        cross(i).wait_send()

        @pl.when(i < Z - 1)
        def _():
            arrival_of = remote(zs.at[i], zr.at[0, 0], z_s.at[i], z_r.at[0, 0], fs=other)
            arrival_of.wait_send()

        return 0

    lax.fori_loop(0, Z, drain, 0)
    last.wait()
    turned[...] = outt[...].astype(jnp.float32).T
    rows = block // 2
    out[...] = turned[pl.ds(c * rows, rows)].astype(jnp.bfloat16)


def run_combine(FS, TP, ht, wd):
    Z = FS // 2
    ff, tokens = ht.shape
    block = tokens // Z
    feats = wd.shape[2]
    vmem = pl.BlockSpec(memory_space=pltpu.VMEM)
    return pl.pallas_call(
        functools.partial(combine, FS, TP, 4, 2),
        out_shape=jax.ShapeDtypeStruct((block // 2, feats), jnp.bfloat16),
        in_specs=[vmem] * 2,
        out_specs=vmem,
        scratch_shapes=[
            pltpu.VMEM((feats, TP * ff), jnp.bfloat16),
            pltpu.VMEM((Z, TP, ff, block), jnp.bfloat16),
            pltpu.VMEM((Z, feats, block), jnp.float32),
            pltpu.VMEM((Z, feats // 2, block), jnp.float32),
            pltpu.VMEM((Z - 1, feats // 2, block), jnp.bfloat16),
            pltpu.VMEM((2, Z // 2, feats // 2, block), jnp.bfloat16),
            pltpu.VMEM((feats, block), jnp.bfloat16),
            pltpu.VMEM((block, feats), jnp.float32),
            DMA((Z,)), DMA((2, Z)), DMA((2, Z)), DMA((2, Z)), DMA((2, Z)),
            DMA((Z,)), DMA((Z,)), DMA((Z - 1,)), DMA((2, Z // 2)), DMA, DMA,
        ],
        compiler_params=pltpu.CompilerParams(collective_id=1, has_side_effects=True, vmem_limit_bytes=20 << 20),
        cost_estimate=pl.CostEstimate(flops=10**9, bytes_accessed=30 << 20, transcendentals=0),
        name="combine",
    )(ht, wd)


def body(FS, TP, tokens, routes, route_logits, gain, w_gate, w_up, w_down):
    gu, ds, tok, wall = run_hand_over(
        FS, TP, tokens, routes.T, route_logits.T, gain[None], w_gate, w_up, w_down
    )
    hidden, gate_t, up_t = run_expert(gu, tok, wall)
    mixed = run_combine(FS, TP, hidden, w_down)
    return (gate_t.T[None], up_t.T[None], ds.reshape(1, 2 * ds.shape[1], -1), mixed)


def solution(mesh):
    return jax.shard_map(
        functools.partial(body, mesh.shape["fs"], mesh.shape["tp"]),
        mesh=mesh,
        in_specs=(
            P(("grp", "fs"), None),
            P(("grp", "fs"), None),
            P(("grp", "fs"), None),
            P("fs"),
            P(None, "fs", "tp"),
            P(None, "fs", "tp"),
            P(None, "fs", "tp"),
        ),
        out_specs=(
            P(("grp", "tp"), None, "fs"),
            P(("grp", "tp"), None, "fs"),
            P(("grp", "tp"), "fs", None),
            P(("grp", "fs"), "tp"),
        ),
        check_vma=False,
    )
```

time: 183 us -> 169 us (0.923)
  Pallas kernels: 172 us -> 159 us
  other arithmetic: 4.76 us -> 0 us
  local copies, waits for them, and re-layouts: 5.34 us -> 9.01 us
    pallas_call x2, Pallas kernels: 164 us -> 150 us  [the longest x1 100 us: run_hand_over(): pl.pallas_call(functools.partial(hand_over, FS, TP), out_shape=(jax.Shape...]
    unnamed x4 -> x18, local copies, waits for them, and re-layouts: 1.56 us -> 9.01 us
    convert_element_type x3 -> x0, other arithmetic: 3.48 us -> none  [the longest x1 1.65 us: mine(): part = (part * scale[None, :, None]).astype(jnp.bfloat16)]
where the time goes in v4:
time: 169 us
  Pallas kernels  159 us (94%)
  local copies, waits for them, and re-layouts  9.01 us (5%)
    pallas_call x1, Pallas kernels, run_hand_over(): pl.pallas_call(functools.partial(hand_over, FS, TP), out_shape=(jax.Shape...  100 us
    pallas_call x1, Pallas kernels, run_combine(): pl.pallas_call(functools.partial(combine, FS, TP, 4, 2), out_shape=jax.Sh...  49.6 us
    pallas_call x1, Pallas kernels, run_expert(): pl.pallas_call(functools.partial(expert, 256), out_shape=(jax.ShapeDtypeS...  9.22 us
    unnamed x18, local copies, waits for them, and re-layouts  9.01 us

profile of v4, /device:TPU:33, one launch (start us, length us, event | category | flops | bytes accessed | tf_op | source)
XLA Modules:
  0.0 168.9 jit_solution(10957686175634941576)
XLA Ops:
  0.6 0.0 copy-start
  0.6 1.5 copy-done
  2.1 0.0 copy-start.1
  2.1 1.5 copy-done.1
  3.6 0.0 copy-start.2
  3.6 1.5 copy-done.2
  5.1 0.0 copy-start.4
  5.1 0.9 copy-done.4
  6.1 0.0 copy-start.5
  6.1 0.7 copy-done.5
  6.8 0.0 copy-start.6
  6.8 0.7 copy-done.6
  7.4 0.0 copy-start.7
  7.4 0.7 copy-done.7
  8.1 100.4 %hand_over.1 = (bf16[32,2,16,896]{3,2,1,0:T(8,128)(2,1)S(1)}, bf16[2,112,2048]{2,1,0:T(8,128)(2,1)S(1)}, bf16[32,64,2048]{2,1,0:T(8,128)(2,1)S(1)}, bf16[32,16,128]{2,1,0:T(8,128)(2,1)S(1)}) custom-call(bf16[64,2048]{1,0:T(8,128)(2,1)S(1)} %copy-done.4, s32[2,64]{1,0:T(2,128)S(1)} %bitcast.11, f32[2,64]{1,0:T(2,128)S(1)} %bitcast.12, f32[1,64]{1,0:T(1,128)S(1)} %bitcast.13, ...), custom_call_target="tpu_custom_call" | custom-call | flops 1000000000 | bytes 31457280 | tf_op jit(solution)/shard_map/hand_over/pallas_call | solution.py:379
  108.5 0.0 copy-start.3
  108.5 9.2 %expert.1 = (bf16[224,2048]{1,0:T(8,128)(2,1)S(1)}, bf16[224,2048]{1,0:T(8,128)(2,1)}, bf16[224,2048]{1,0:T(8,128)(2,1)}) custom-call(bf16[32,2,16,896]{3,2,1,0:T(8,128)(2,1)S(1)} %get-tuple-element.11.gu, bf16[32,64,2048]{2,1,0:T(8,128)(2,1)S(1)} %get-tuple-element.12.x, bf16[32,16,128]{2,1,0:T(8,128)(2,1)S(1)} %get-tuple-element.13.w), custom_call_target="tpu_custom_call" | custom-call | flops 4000000000 | bytes 16777216 | tf_op jit(solution)/shard_map/expert/pallas_call | solution.py:453
  117.7 0.0 copy-done.3
  117.7 49.6 %combine.1 = bf16[64,512]{1,0:T(8,128)(2,1)S(1)} custom-call(bf16[224,2048]{1,0:T(8,128)(2,1)S(1)} %get-tuple-element.17.ht, f32[4,224,512]{2,1,0:T(8,128)S(1)} %copy-done.3), custom_call_target="tpu_custom_call" | custom-call | flops 1000000000 | bytes 31457280 | tf_op jit(solution)/shard_map/combine/pallas_call | solution.py:614
  167.3 0.9 copy.13
  168.2 0.6 copy.14
Async XLA Ops:
  0.6 1.5 copy-start
  2.1 1.5 copy-start.1
  3.6 1.5 copy-start.2
  5.1 0.9 copy-start.4
  6.1 0.7 copy-start.5
  6.8 0.7 copy-start.6
  7.4 0.7 copy-start.7
  108.5 9.2 %copy-start.3 = (f32[4,224,512]{2,1,0:T(8,128)S(1)}, f32[4,224,512]{2,1,0:T(8,128)}, u32[]{:S(2)}) copy-start(f32[4,224,512]{2,1,0:T(8,128)} %wd.1) | copy-start | bytes 5505028

commit v5 on v4

--- a/solution.py
+++ b/solution.py
@@ -19,8 +19,8 @@
 
 
 def hand_over(
-    FS, TP, x_in, routes, logits, gain, w_gate, w_up, w_down, gu, ds, tok, wall,
-    raw_gate, raw_up, raw_down, scale, wp, dn, nt, wt, xr, stage,
+    FS, TP, x_hbm, routes_hbm, logits_hbm, gain_hbm, w_gate, w_up, w_down, gu, ds, tok, wall,
+    x_in, routes, logits, gain, raw_gate, raw_up, raw_down, scale, wp, dn, nt, wt, xr, stage,
     in_s, loc, xw_s, xw_r, st_s, st_r, sf_s, sf_r, xd_s, xd_r, rs, rr, ws, wr, xt_s, xt_r, xo_s, xo_r,
     cc_s, cc_r, cw_s, cw_r, za_s, za_r, y_s, y_r, yd_s, yd_r,
 ):
@@ -44,6 +44,10 @@
     opposite = (x + 2) % TP
 
     fetch = (
+        pltpu.make_async_copy(x_hbm, x_in, in_s.at[3]),
+        pltpu.make_async_copy(routes_hbm, routes, in_s.at[4]),
+        pltpu.make_async_copy(logits_hbm, logits, in_s.at[5]),
+        pltpu.make_async_copy(gain_hbm, gain, in_s.at[6]),
         pltpu.make_async_copy(w_gate.at[:, pl.ds(p * rows, rows)], raw_gate, in_s.at[0]),
         pltpu.make_async_copy(w_up.at[:, pl.ds(p * rows, rows)], raw_up, in_s.at[1]),
         pltpu.make_async_copy(w_down.at[:, pl.ds(p * drows, drows)], raw_down, in_s.at[2]),
@@ -62,6 +66,8 @@
         pl.semaphore_signal(barrier, inc=1, device_id={"tp": (x + k) % TP}, device_id_type=MESH)
     pl.semaphore_signal(barrier, inc=1, device_id={"grp": mate}, device_id_type=MESH)
 
+    for copy in fetch[:4]:
+        copy.wait()
     values = x_in[...].astype(jnp.float32)
     mean_square = jnp.mean(values * values, axis=-1, keepdims=True)
     nt[...] = (values * lax.rsqrt(mean_square + 1e-06)).astype(jnp.bfloat16)
@@ -75,22 +81,18 @@
     factor = scale[pl.ds(p * rows, rows), :][:, :1]
     ff = wp.shape[4] // 4
     part = rows // 2
-    fetch[0].wait()
-    fetch[1].wait()
-
-    def pack(e, _):
+    fetch[4].wait()
+    fetch[5].wait()
+
+    def pack(e):
         gate = raw_gate[e] * factor
         up = raw_up[e] * factor
         for j in range(2 * Q):
             span = slice(j * ff, (j + 1) * ff)
             quarters = [gate[:part, span], up[:part, span], gate[part:, span], up[part:, span]]
             wp[e, j // 2, j % 2] = jnp.concatenate(quarters, axis=1).astype(jnp.bfloat16)
-        return 0
-
-    lax.fori_loop(0, TP, pack, 0)
-    fetch[2].wait()
-    dn[...] = raw_down[...].astype(jnp.bfloat16)
-
+
+    pack(opposite)
     pl.semaphore_wait(barrier, FS - 1 + TP - 1 + 1)
 
     def cols(i):
@@ -135,10 +137,32 @@
         held = ds.at[p, :, dcols((x + TP - k) % TP)]
         return remote(held, held, xd_s.at[k - 1], xd_r.at[k - 1], tp=(x + k) % TP)
 
-    for n in range(Q):
-        first_leg(n).start()
-        for side in (0, 1):
-            xw(n, side).start()
+    def send_packed(k, _):
+        @pl.when(k == 0)
+        def _():
+            first_leg(0).start()
+            first_leg(1).start()
+
+        e = jnp.where(k < 2, jnp.where(k == 0, xside[0], xside[1]), x)
+        pack(e)
+
+        @pl.when(k == 0)
+        def _():
+            for n in range(Q):
+                xw(n, 0).start()
+
+        @pl.when(k == 1)
+        def _():
+            for n in range(Q):
+                xw(n, 1).start()
+            for n in range(2, Q):
+                first_leg(n).start()
+
+        return 0
+
+    lax.fori_loop(0, 3, send_packed, 0)
+    fetch[6].wait()
+    dn[...] = raw_down[...].astype(jnp.bfloat16)
     own_cross = remote(nt, tok.at[f], cc_s.at[Z - 1], cc_r.at[Z - 1], fs=other)
     own_cross.start()
     own_cross_w = remote(wt, wall.at[f], cw_s.at[Z - 1], cw_r.at[Z - 1], fs=other)
@@ -372,7 +396,7 @@
     half = rows // 2
     drows, db = w_down.shape[1] // 2, w_down.shape[2]
     vmem = pl.BlockSpec(memory_space=pltpu.VMEM)
-    hbm = pl.BlockSpec(memory_space=pl.ANY)
+    hbm = pl.BlockSpec(memory_space=pltpu.HBM)
     tile = (16, LANES)
     piece = (half // 2, 4 * ff)
     bf16 = jnp.bfloat16
@@ -384,9 +408,13 @@
             jax.ShapeDtypeStruct((FS,) + tokens.shape, bf16),
             jax.ShapeDtypeStruct((FS,) + tile, bf16),
         ),
-        in_specs=[vmem] * 4 + [hbm] * 3,
+        in_specs=[hbm] * 7,
         out_specs=(vmem,) * 4,
         scratch_shapes=[
+            pltpu.VMEM(tokens.shape, tokens.dtype),
+            pltpu.VMEM(routes.shape, routes.dtype),
+            pltpu.VMEM(logits.shape, logits.dtype),
+            pltpu.VMEM(gain.shape, gain.dtype),
             pltpu.VMEM((TP, half, w_gate.shape[2]), jnp.float32),
             pltpu.VMEM((TP, half, w_gate.shape[2]), jnp.float32),
             pltpu.VMEM((TP, drows, db), jnp.float32),
@@ -397,7 +425,7 @@
             pltpu.VMEM(tile, bf16),
             pltpu.VMEM((TP, Q, 2) + piece, bf16),
             pltpu.VMEM((Q, 2) + piece, bf16),
-            DMA((3,)), DMA((5,)),
+            DMA((7,)), DMA((5,)),
             DMA((2, Q)), DMA((2, Q)), DMA((Q,)), DMA((Q,)), DMA((Q,)), DMA((Q,)),
             DMA((TP - 1,)), DMA((TP - 1,)),
             DMA((2, Z // 2)), DMA((2, Z // 2)), DMA((2, Z // 2)), DMA((2, Z // 2)),
@@ -409,16 +437,17 @@
         compiler_params=pltpu.CompilerParams(collective_id=0, has_side_effects=True, vmem_limit_bytes=16 << 20),
         cost_estimate=pl.CostEstimate(flops=10**9, bytes_accessed=30 << 20, transcendentals=0),
         name="hand_over",
-    )(tokens, routes, logits, gain, w_gate, w_up, w_down)
-
-
-def expert(block, gu, x, w, ht, gate_out, up_out, wg, wu):
-    features = x.shape[2]
-    count = block // x.shape[1]
+    )(*[
+        pltpu.with_memory_space_constraint(a, pltpu.HBM)
+        for a in (tokens, routes, logits, gain, w_gate, w_up, w_down)
+    ])
+
+
+def unpack(block, gu, wg, wu, gate_out, up_out):
     part, ff = gu.shape[2], gu.shape[3] // 4
     pieces = block // (2 * part)
 
-    def unpack(i, _):
+    def step(i, _):
         span = pl.ds(pl.multiple_of(i * block, block), block)
         for v in range(pieces):
             k = i * pieces + v
@@ -431,42 +460,31 @@
             served[:, span] = own[span, :].astype(jnp.float32).T.astype(jnp.bfloat16)
         return 0
 
-    lax.fori_loop(0, features // block, unpack, 0)
-
-    def step(i, _):
-        span = pl.ds(pl.multiple_of(i * block, block), block)
-        rows = x[pl.ds(i * count, count)].reshape(block, features)
-        gate = jnp.dot(rows, wg[...], preferred_element_type=jnp.float32)
-        up = jnp.dot(rows, wu[...], preferred_element_type=jnp.float32)
-        scale = jnp.concatenate([w[i * count + n, 0:1, : x.shape[1]] for n in range(count)], axis=1)
-        ht[:, span] = ((jax.nn.silu(gate) * up).T * scale.astype(jnp.float32)).astype(jnp.bfloat16)
-        return 0
-
-    lax.fori_loop(0, x.shape[0] // count, step, 0)
-
-
-def run_expert(gu, x, w):
-    tokens, features = x.shape[0] * x.shape[1], x.shape[2]
+    lax.fori_loop(0, wg.shape[0] // block, step, 0)
+
+
+def run_unpack(gu):
     ff = gu.shape[3] // 4
+    features = gu.shape[0] * gu.shape[1] * gu.shape[2] * 2
     vmem = pl.BlockSpec(memory_space=pltpu.VMEM)
     bf16 = jnp.bfloat16
     return pl.pallas_call(
-        functools.partial(expert, 256),
+        functools.partial(unpack, 256),
         out_shape=(
-            jax.ShapeDtypeStruct((ff, tokens), bf16),
+            jax.ShapeDtypeStruct((features, ff), bf16),
+            jax.ShapeDtypeStruct((features, ff), bf16),
             jax.ShapeDtypeStruct((ff, features), bf16),
             jax.ShapeDtypeStruct((ff, features), bf16),
         ),
-        in_specs=[vmem] * 3,
-        out_specs=(vmem,) * 3,
-        scratch_shapes=[pltpu.VMEM((features, ff), bf16), pltpu.VMEM((features, ff), bf16)],
-        compiler_params=pltpu.CompilerParams(vmem_limit_bytes=12 << 20),
-        cost_estimate=pl.CostEstimate(flops=4 * 10**9, bytes_accessed=16 << 20, transcendentals=0),
-        name="expert",
-    )(gu, x, w)
-
-
-def combine(FS, TP, W, L, ht, wd, out, wdt, hs, part, prec, zs, zr, outt, turned, loc, xd_s, xd_r, xo_s, xo_r, cc_s, cc_r, z_s, z_r, fin_s, fin_r):
+        in_specs=[vmem],
+        out_specs=(vmem,) * 4,
+        compiler_params=pltpu.CompilerParams(vmem_limit_bytes=8 << 20),
+        cost_estimate=pl.CostEstimate(flops=10**9, bytes_accessed=16 << 20, transcendentals=0),
+        name="unpack",
+    )(gu)
+
+
+def combine(FS, TP, L, wg, wu, tok, wall, wd, out, wdt, hs, part, prec, zs, zr, outt, turned, xd_s, xd_r, xo_s, xo_r, cc_s, cc_r, z_s, z_r, fin_s, fin_r):
     Z = FS // 2
     H = Z // 2
     x, f = lax.axis_index("tp"), lax.axis_index("fs")
@@ -483,7 +501,6 @@
         pl.semaphore_signal(barrier, inc=1, device_id={"tp": k}, device_id_type=MESH)
     for k in zside + (other,):
         pl.semaphore_signal(barrier, inc=1, device_id={"fs": k}, device_id_type=MESH)
-    pl.semaphore_wait(barrier, 5)
 
     def away(i):
         return H - (i + 1) // 2
@@ -491,19 +508,33 @@
     def chip(i):
         return jnp.where(i % 2 == 0, (z + away(i)) % Z, (z + Z - away(i)) % Z)
 
-    def mine(i):
-        return ht.at[:, pl.ds(pl.multiple_of(chip(i) * block, LANES), block)]
-
-    def keep_own(i):
-        return pltpu.make_async_copy(mine(i), hs.at[i, x], loc.at[i])
+    count, features = tok.shape[1], tok.shape[2]
+
+    def make(i):
+        rows = jnp.concatenate([tok[pl.ds(2 * chip(i + v), 2)].reshape(block, features) for v in (0, 1)], axis=0)
+        gate = jnp.dot(rows, wg[...], preferred_element_type=jnp.float32)
+        up = jnp.dot(rows, wu[...], preferred_element_type=jnp.float32)
+        hidden = (jax.nn.silu(gate) * up).T
+        for v in (0, 1):
+            scale = [wall[2 * chip(i + v) + n, 0:1, :count] for n in (0, 1)]
+            scale = jnp.concatenate(scale, axis=1).astype(jnp.float32)
+            hs[i + v, x] = (hidden[:, v * block : (v + 1) * block] * scale).astype(jnp.bfloat16)
 
     def direct(i, side):
-        return remote(mine(i), hs.at[i, x], xd_s.at[side, i], xd_r.at[side, i], tp=xside[side])
+        return remote(hs.at[i, x], hs.at[i, x], xd_s.at[side, i], xd_r.at[side, i], tp=xside[side])
+
+    def direct_recv(i, side):
+        held = hs.at[i, xside[1 - side]]
+        return remote(held, held, xd_s.at[side, i], xd_r.at[side, i], tp=xside[side])
 
     def onward(i, side):
         held = hs.at[i, xside[1 - side], pl.ds(side * half, half)]
         return remote(held, held, xo_s.at[side, i], xo_r.at[side, i], tp=xside[side])
 
+    def onward_recv(i, side):
+        held = hs.at[i, (x + 2) % TP, pl.ds(side * half, half)]
+        return remote(held, held, xo_s.at[side, i], xo_r.at[side, i], tp=xside[side])
+
     def cross(j):
         return remote(part.at[j, pl.ds((1 - c) * keep, keep)], prec.at[j], cc_s.at[j], cc_r.at[j], fs=other)
 
@@ -514,35 +545,48 @@
     def arrival(side, k):
         return remote(zs.at[0], zr.at[side, k], z_s.at[0], z_r.at[side, k], fs=zside[side])
 
-    def own_first(i, _):
-        keep_own(i).start()
-        return 0
-
-    lax.fori_loop(0, Z, own_first, 0)
-    for i in range(W):
-        for side in (0, 1):
-            direct(i, side).start()
+    AHEAD = 4
+
+    def begin(k, _):
+        make(2 * k)
+
+        @pl.when(k == 0)
+        def _():
+            pl.semaphore_wait(barrier, 5)
+
+        @pl.when(2 * k < AHEAD)
+        def _():
+            for v in (0, 1):
+                for side in (0, 1):
+                    direct(2 * k + v, side).start()
+
+        return 0
+
+    lax.fori_loop(0, AHEAD // 2 + 1, begin, 0)
     for e in range(TP):
         wdt[:, e * ff : (e + 1) * ff] = wd[e].T.astype(jnp.bfloat16)
 
     def step(i, _):
-        @pl.when(i + W < Z)
+        @pl.when(i + AHEAD < Z)
         def _():
             for side in (0, 1):
-                direct(i + W, side).start()
+                direct(i + AHEAD, side).start()
 
         @pl.when(i < Z)
         def _():
             for side in (0, 1):
-                direct(i, side).wait_recv()
+                direct_recv(i, side).wait_recv()
                 onward(i, side).start()
 
+        @pl.when((i % 2 == 0) & (i + AHEAD + 2 < Z))
+        def _():
+            make(i + AHEAD + 2)
+
         @pl.when((i >= L) & (i < Z + L))
         def _():
             j = i - L
-            keep_own(j).wait()
             for side in (0, 1):
-                onward(j, side).wait_recv()
+                onward_recv(j, side).wait_recv()
             rhs = hs[j].reshape(TP * ff, block)
             part[j] = jnp.dot(wdt[...], rhs, preferred_element_type=jnp.float32)
             cross(j).start()
@@ -605,16 +649,16 @@
     out[...] = turned[pl.ds(c * rows, rows)].astype(jnp.bfloat16)
 
 
-def run_combine(FS, TP, ht, wd):
+def run_combine(FS, TP, wg, wu, tok, wall, wd):
     Z = FS // 2
-    ff, tokens = ht.shape
-    block = tokens // Z
+    ff = wg.shape[1]
+    block = 2 * tok.shape[1]
     feats = wd.shape[2]
     vmem = pl.BlockSpec(memory_space=pltpu.VMEM)
     return pl.pallas_call(
-        functools.partial(combine, FS, TP, 4, 2),
+        functools.partial(combine, FS, TP, 2),
         out_shape=jax.ShapeDtypeStruct((block // 2, feats), jnp.bfloat16),
-        in_specs=[vmem] * 2,
+        in_specs=[vmem] * 5,
         out_specs=vmem,
         scratch_shapes=[
             pltpu.VMEM((feats, TP * ff), jnp.bfloat16),
@@ -625,21 +669,21 @@
             pltpu.VMEM((2, Z // 2, feats // 2, block), jnp.bfloat16),
             pltpu.VMEM((feats, block), jnp.bfloat16),
             pltpu.VMEM((block, feats), jnp.float32),
-            DMA((Z,)), DMA((2, Z)), DMA((2, Z)), DMA((2, Z)), DMA((2, Z)),
+            DMA((2, Z)), DMA((2, Z)), DMA((2, Z)), DMA((2, Z)),
             DMA((Z,)), DMA((Z,)), DMA((Z - 1,)), DMA((2, Z // 2)), DMA, DMA,
         ],
         compiler_params=pltpu.CompilerParams(collective_id=1, has_side_effects=True, vmem_limit_bytes=20 << 20),
         cost_estimate=pl.CostEstimate(flops=10**9, bytes_accessed=30 << 20, transcendentals=0),
         name="combine",
-    )(ht, wd)
+    )(wg, wu, tok, wall, wd)
 
 
 def body(FS, TP, tokens, routes, route_logits, gain, w_gate, w_up, w_down):
     gu, ds, tok, wall = run_hand_over(
         FS, TP, tokens, routes.T, route_logits.T, gain[None], w_gate, w_up, w_down
     )
-    hidden, gate_t, up_t = run_expert(gu, tok, wall)
-    mixed = run_combine(FS, TP, hidden, w_down)
+    wg, wu, gate_t, up_t = run_unpack(gu)
+    mixed = run_combine(FS, TP, wg, wu, tok, wall, w_down)
     return (gate_t.T[None], up_t.T[None], ds.reshape(1, 2 * ds.shape[1], -1), mixed)
 
 

time: 169 us -> 155 us (0.917)
  local copies, waits for them, and re-layouts: 9.01 us -> 1.56 us
  Pallas kernels: 159 us -> 153 us
    unnamed x18 -> x4, local copies, waits for them, and re-layouts: 9.01 us -> 1.56 us
    pallas_call x2, Pallas kernels: 58.8 us -> 53.2 us  [the longest x1 49.7 us: run_combine(): pl.pallas_call(functools.partial(combine, FS, TP, 2), out_shape=jax.Shape...]
where the time goes in v5:
time: 155 us
  Pallas kernels  153 us (99%)
  local copies, waits for them, and re-layouts  1.56 us (1%)
    pallas_call x1, Pallas kernels, run_hand_over(): pl.pallas_call(functools.partial(hand_over, FS, TP), out_shape=(jax.Shape...  99.8 us
    pallas_call x1, Pallas kernels, run_combine(): pl.pallas_call(functools.partial(combine, FS, TP, 2), out_shape=jax.Shape...  49.7 us
    pallas_call x1, Pallas kernels, run_unpack(): pl.pallas_call(functools.partial(unpack, 256), out_shape=(jax.ShapeDtypeS...  3.56 us

profile of v5, /device:TPU:33, one launch (start us, length us, event | category | flops | bytes accessed | tf_op | source)
XLA Modules:
  0.0 155.2 jit_solution(9995998940769398393)
XLA Ops:
  0.6 99.8 %hand_over.1 = (bf16[32,2,16,896]{3,2,1,0:T(8,128)(2,1)S(1)}, bf16[2,112,2048]{2,1,0:T(8,128)(2,1)S(1)}, bf16[32,64,2048]{2,1,0:T(8,128)(2,1)S(1)}, bf16[32,16,128]{2,1,0:T(8,128)(2,1)S(1)}) custom-call(bf16[64,2048]{1,0:T(8,128)(2,1)} %x_hbm.1, s32[2,64]{1,0:T(2,128)} %bitcast.11, f32[2,64]{1,0:T(2,128)} %bitcast.12, f32[1,64]{1,0:T(1,128)} %bitcast.13, ...), custom_call_target="tpu_custom_call" | custom-call | flops 1000000000 | bytes 31457280 | tf_op jit(solution)/shard_map/hand_over/pallas_call | solution.py:403
  100.4 0.0 copy-start
  100.4 3.6 %unpack.1 = (bf16[2048,224]{1,0:T(8,128)(2,1)S(1)}, bf16[2048,224]{1,0:T(8,128)(2,1)S(1)}, bf16[224,2048]{1,0:T(8,128)(2,1)}, bf16[224,2048]{1,0:T(8,128)(2,1)}) custom-call(bf16[32,2,16,896]{3,2,1,0:T(8,128)(2,1)S(1)} %get-tuple-element.12.gu), custom_call_target="tpu_custom_call" | custom-call | flops 1000000000 | bytes 16777216 | tf_op jit(solution)/shard_map/unpack/pallas_call | solution.py:471
  104.0 0.0 copy-done
  104.0 49.7 %combine.1 = bf16[64,512]{1,0:T(8,128)(2,1)S(1)} custom-call(bf16[2048,224]{1,0:T(8,128)(2,1)S(1)} %get-tuple-element.16.wg, bf16[2048,224]{1,0:T(8,128)(2,1)S(1)} %get-tuple-element.17.wu, bf16[32,64,2048]{2,1,0:T(8,128)(2,1)S(1)} %get-tuple-element.18.tok, bf16[32,16,128]{2,1,0:T(8,128)(2,1)S(1)} %get-tuple-element.19.wall, f32[4,224,512]{2,1,0:T(8,128)S(1)} %copy-done), custom_call_target="tpu_custom_call" | custom-call | flops 1000000000 | bytes 31457280 | tf_op jit(solution)/shard_map/combine/pallas_call | solution.py:658
  153.7 0.9 copy.13
  154.6 0.6 copy.14
Async XLA Ops:
  100.4 3.6 %copy-start = (f32[4,224,512]{2,1,0:T(8,128)S(1)}, f32[4,224,512]{2,1,0:T(8,128)}, u32[]{:S(2)}) copy-start(f32[4,224,512]{2,1,0:T(8,128)} %wd.1) | copy-start | bytes 5505028

commit v6 on v5

--- a/solution.py
+++ b/solution.py
@@ -20,9 +20,9 @@
 
 def hand_over(
     FS, TP, x_hbm, routes_hbm, logits_hbm, gain_hbm, w_gate, w_up, w_down, gu, ds, tok, wall,
-    x_in, routes, logits, gain, raw_gate, raw_up, raw_down, scale, wp, dn, nt, wt, xr, stage,
+    x_in, routes, logits, gain, raw_gate, raw_up, raw_down, scale, wp, dn, nt, wt, xr, stage, relay,
     in_s, loc, xw_s, xw_r, st_s, st_r, sf_s, sf_r, xd_s, xd_r, rs, rr, ws, wr, xt_s, xt_r, xo_s, xo_r,
-    cc_s, cc_r, cw_s, cw_r, za_s, za_r, y_s, y_r, yd_s, yd_r,
+    cc_s, cc_r, cw_s, cw_r, za_s, za_r, ra_s, ra_r, rb_s, y_s, y_r, yd_s, yd_r,
 ):
     Z = FS // 2
     H = Z // 2
@@ -222,6 +222,18 @@
         held = gu.at[2 * source(n, u) + cs, p]
         return remote(held, held, za_s.at[n * TP + u, cs], za_r.at[n * TP + u, cs], fs=other)
 
+    def half_way(side):
+        return (z + Q) % Z if side == 0 else (z + Z - Q) % Z
+
+    def relay_out(side):
+        zc = (z + H) % Z
+        piece = xr.at[zc // Q, seat, side]
+        return remote(piece, relay.at[side], ra_s.at[side], ra_r.at[side], fs=half_way(side) * 2 + c)
+
+    def relay_on(side):
+        fo = half_way(1 - side) * 2 + c
+        return remote(relay.at[side], gu.at[fo, p], rb_s.at[side], za_r.at[2, c], fs=half_way(side) * 2 + side)
+
     def y_hand(n, u):
         held = gu.at[pl.ds(2 * source(n, u), 2), p]
         return remote(held, held, y_s.at[n * TP + u], y_r.at[n * TP + u], grp=mate)
@@ -242,6 +254,9 @@
             if n == 0 and u == 0:
                 za(0, 0, 1 - c).start()
                 own.start()
+            elif n == 0 and u == 2:
+                relay_out(0).start()
+                relay_out(1).start()
             else:
                 za(n, u, 0).start()
                 za(n, u, 1).start()
@@ -300,16 +315,18 @@
         second_leg(n).start()
     for k in (2, 1, 3):
         xd(k).start()
-    ring_step(2)
     local[0].wait()
     issue(0)
-    for s in range(3, H + 1):
+    for s in range(2, H + 1):
         ring_step(s)
-        issue(s - 2)
-        if s == H:
-            issue(s - 1)
-        for i in (2 * s - 6, 2 * s - 5):
-            pass_on(i)
+        issue(s - 1)
+        if s == 3:
+            for side in (0, 1):
+                relay_out(side).wait_recv()
+                relay_on(side).start()
+        if s > 2:
+            for i in (2 * s - 6, 2 * s - 5):
+                pass_on(i)
         if s == 4:
             local[1].wait()
             for k in (2, 1, 3):
@@ -318,18 +335,18 @@
         if s > 3:
             for i in (2 * s - 8, 2 * s - 7):
                 finish(i)
-            accept(s - 4)
+        if s > 2:
+            accept(s - 3)
     pass_on(2 * H - 4)
     pass_on(2 * H - 3)
     finish(2 * H - 6)
     finish(2 * H - 5)
-    accept(H - 3)
+    accept(H - 2)
     pass_on(2 * H - 2)
     finish(2 * H - 4)
     finish(2 * H - 3)
-    accept(H - 2)
+    accept(H - 1)
     finish(2 * H - 2)
-    accept(H - 1)
 
     local[2].wait()
     local[3].wait()
@@ -370,13 +387,19 @@
 
     def exchange_drain(v, _):
         n, u = v // TP, v % TP
-        za(n, u, 0).wait_send()
-        za(n, u, 1).wait_send()
+        @pl.when(v != 2)
+        def _():
+            za(n, u, 0).wait_send()
+            za(n, u, 1).wait_send()
+
         y_hand(n, u).wait_send()
         y_recv(n, u).wait_recv()
         return 0
 
     lax.fori_loop(1, Z, exchange_drain, 0)
+    for side in (0, 1):
+        relay_out(side).wait_send()
+        relay_on(side).wait_send()
     yd.wait_send()
     remote(ds.at[1 - p], ds.at[1 - p], yd_s, yd_r, grp=mate).wait_recv()
     for n in range(Q):
@@ -425,13 +448,14 @@
             pltpu.VMEM(tile, bf16),
             pltpu.VMEM((TP, Q, 2) + piece, bf16),
             pltpu.VMEM((Q, 2) + piece, bf16),
+            pltpu.VMEM((2,) + piece, bf16),
             DMA((7,)), DMA((5,)),
             DMA((2, Q)), DMA((2, Q)), DMA((Q,)), DMA((Q,)), DMA((Q,)), DMA((Q,)),
             DMA((TP - 1,)), DMA((TP - 1,)),
             DMA((2, Z // 2)), DMA((2, Z // 2)), DMA((2, Z // 2)), DMA((2, Z // 2)),
             DMA((2, Z - 1)), DMA((2, Z - 1)), DMA((2, Z - 1)), DMA((2, Z - 1)),
             DMA((Z,)), DMA((Z,)), DMA((Z,)), DMA((Z,)),
-            DMA((Z, 2)), DMA((Z, 2)),
+            DMA((Z, 2)), DMA((Z, 2)), DMA((2,)), DMA((2,)), DMA((2,)),
             DMA((Z,)), DMA((Z,)), DMA, DMA,
         ],
         compiler_params=pltpu.CompilerParams(collective_id=0, has_side_effects=True, vmem_limit_bytes=16 << 20),
@@ -443,7 +467,9 @@
     ])
 
 
-def unpack(block, gu, wg, wu, gate_out, up_out):
+def unpack(block, gu, ds, wg, wu, gate_out, up_out, down_out, sem):
+    down = pltpu.make_async_copy(ds, down_out, sem)
+    down.start()
     part, ff = gu.shape[2], gu.shape[3] // 4
     pieces = block // (2 * part)
 
@@ -461,9 +487,10 @@
         return 0
 
     lax.fori_loop(0, wg.shape[0] // block, step, 0)
-
-
-def run_unpack(gu):
+    down.wait()
+
+
+def run_unpack(gu, ds):
     ff = gu.shape[3] // 4
     features = gu.shape[0] * gu.shape[1] * gu.shape[2] * 2
     vmem = pl.BlockSpec(memory_space=pltpu.VMEM)
@@ -475,13 +502,15 @@
             jax.ShapeDtypeStruct((features, ff), bf16),
             jax.ShapeDtypeStruct((ff, features), bf16),
             jax.ShapeDtypeStruct((ff, features), bf16),
+            jax.ShapeDtypeStruct(ds.shape, bf16),
         ),
-        in_specs=[vmem],
-        out_specs=(vmem,) * 4,
+        in_specs=[vmem] * 2,
+        out_specs=(vmem,) * 4 + (pl.BlockSpec(memory_space=pltpu.HBM),),
+        scratch_shapes=[DMA],
         compiler_params=pltpu.CompilerParams(vmem_limit_bytes=8 << 20),
         cost_estimate=pl.CostEstimate(flops=10**9, bytes_accessed=16 << 20, transcendentals=0),
         name="unpack",
-    )(gu)
+    )(gu, ds)
 
 
 def combine(FS, TP, L, wg, wu, tok, wall, wd, out, wdt, hs, part, prec, zs, zr, outt, turned, xd_s, xd_r, xo_s, xo_r, cc_s, cc_r, z_s, z_r, fin_s, fin_r):
@@ -545,7 +574,7 @@
     def arrival(side, k):
         return remote(zs.at[0], zr.at[side, k], z_s.at[0], z_r.at[side, k], fs=zside[side])
 
-    AHEAD = 4
+    AHEAD = 2
 
     def begin(k, _):
         make(2 * k)
@@ -682,9 +711,9 @@
     gu, ds, tok, wall = run_hand_over(
         FS, TP, tokens, routes.T, route_logits.T, gain[None], w_gate, w_up, w_down
     )
-    wg, wu, gate_t, up_t = run_unpack(gu)
+    wg, wu, gate_t, up_t, down = run_unpack(gu, ds)
     mixed = run_combine(FS, TP, wg, wu, tok, wall, w_down)
-    return (gate_t.T[None], up_t.T[None], ds.reshape(1, 2 * ds.shape[1], -1), mixed)
+    return (gate_t.T[None], up_t.T[None], down.reshape(1, 2 * ds.shape[1], -1), mixed)
 
 
 def solution(mesh):

time: 155 us -> 156 us (level)
  Pallas kernels: 153 us -> 155 us
    pallas_call x1, Pallas kernels: 99.8 us -> 104 us  [run_hand_over(): pl.pallas_call(functools.partial(hand_over, FS, TP), out_shape=(jax.Shape...]
    pallas_call x1, Pallas kernels: 49.7 us -> 47.3 us  [run_combine(): pl.pallas_call(functools.partial(combine, FS, TP, 2), out_shape=jax.Shape...]
where the time goes in v6:
time: 156 us
  Pallas kernels  155 us (99%)
    pallas_call x1, Pallas kernels, run_hand_over(): pl.pallas_call(functools.partial(hand_over, FS, TP), out_shape=(jax.Shape...  104 us
    pallas_call x1, Pallas kernels, run_combine(): pl.pallas_call(functools.partial(combine, FS, TP, 2), out_shape=jax.Shape...  47.3 us
    pallas_call x1, Pallas kernels, run_unpack(): pl.pallas_call(functools.partial(unpack, 256), out_shape=(jax.ShapeDtypeS...  3.6 us

profile of v6, /device:TPU:33, one launch (start us, length us, event | category | flops | bytes accessed | tf_op | source)
XLA Modules:
  0.0 156.0 jit_solution(2260365404570324538)
XLA Ops:
  0.6 103.7 %hand_over.1 = (bf16[32,2,16,896]{3,2,1,0:T(8,128)(2,1)S(1)}, bf16[2,112,2048]{2,1,0:T(8,128)(2,1)S(1)}, bf16[32,64,2048]{2,1,0:T(8,128)(2,1)S(1)}, bf16[32,16,128]{2,1,0:T(8,128)(2,1)S(1)}) custom-call(bf16[64,2048]{1,0:T(8,128)(2,1)} %x_hbm.1, s32[2,64]{1,0:T(2,128)} %bitcast.10, f32[2,64]{1,0:T(2,128)} %bitcast.11, f32[1,64]{1,0:T(1,128)} %bitcast.12, ...), custom_call_target="tpu_custom_call" | custom-call | flops 1000000000 | bytes 31457280 | tf_op jit(solution)/shard_map/hand_over/pallas_call | solution.py:426
  104.4 0.0 copy-start
  104.4 3.6 %unpack.1 = (bf16[2048,224]{1,0:T(8,128)(2,1)S(1)}, bf16[2048,224]{1,0:T(8,128)(2,1)S(1)}, bf16[224,2048]{1,0:T(8,128)(2,1)}, bf16[224,2048]{1,0:T(8,128)(2,1)}, bf16[2,112,2048]{2,1,0:T(8,128)(2,1)}) custom-call(bf16[32,2,16,896]{3,2,1,0:T(8,128)(2,1)S(1)} %get-tuple-element.13.gu, bf16[2,112,2048]{2,1,0:T(8,128)(2,1)S(1)} %get-tuple-element.14.ds), custom_call_target="tpu_custom_call" | custom-call | flops 1000000000 | bytes 16777216 | tf_op jit(solution)/shard_map/unpack/pallas_call | solution.py:498
  108.0 0.0 copy-done
  108.0 47.3 %combine.1 = bf16[64,512]{1,0:T(8,128)(2,1)S(1)} custom-call(bf16[2048,224]{1,0:T(8,128)(2,1)S(1)} %get-tuple-element.18.wg, bf16[2048,224]{1,0:T(8,128)(2,1)S(1)} %get-tuple-element.19.wu, bf16[32,64,2048]{2,1,0:T(8,128)(2,1)S(1)} %get-tuple-element.20.tok, bf16[32,16,128]{2,1,0:T(8,128)(2,1)S(1)} %get-tuple-element.21.wall, f32[4,224,512]{2,1,0:T(8,128)S(1)} %copy-done), custom_call_target="tpu_custom_call" | custom-call | flops 1000000000 | bytes 31457280 | tf_op jit(solution)/shard_map/combine/pallas_call | solution.py:687
  155.4 0.6 copy.12
Async XLA Ops:
  104.4 3.6 %copy-start = (f32[4,224,512]{2,1,0:T(8,128)S(1)}, f32[4,224,512]{2,1,0:T(8,128)}, u32[]{:S(2)}) copy-start(f32[4,224,512]{2,1,0:T(8,128)} %wd.1) | copy-start | bytes 5505028

commit v7 on v5

--- a/solution.py
+++ b/solution.py
@@ -27,10 +27,11 @@
     Z = FS // 2
     H = Z // 2
     Q = Z // TP
-    assert TP == 4 and Q * TP == Z and H == 2 * Q
+    assert TP == 4 and Q == 4 and Q * TP == Z
     x, f, g = lax.axis_index("tp"), lax.axis_index("fs"), lax.axis_index("grp")
     z, c = f // 2, f % 2
     zone, seat = z // Q, z % Q
+    order = (0, 2, 1, 3)
     p = g % 2
     mate = g + 1 - 2 * p
     fb = nt.shape[1] // TP
@@ -114,6 +115,9 @@
     def spot(n):
         return (seat + n) % Q
 
+    def leg(n):
+        return n // 2
+
     def xw(n, side):
         return remote(wp.at[xside[side], spot(n)], xr.at[x, spot(n)], xw_s.at[side, n], xw_r.at[side, n], tp=xside[side])
 
@@ -122,13 +126,13 @@
         return remote(held, held, xw_s.at[side, n], xw_r.at[side, n], tp=xside[side])
 
     def first_leg(n):
-        return remote(wp.at[opposite, spot(n)], stage.at[n], st_s.at[n], st_r.at[n], tp=xside[n % 2])
+        return remote(wp.at[opposite, spot(n)], stage.at[n], st_s.at[n], st_r.at[n], tp=xside[leg(n)])
 
     def second_leg(n):
-        return remote(stage.at[n], xr.at[xside[1 - n % 2], spot(n)], sf_s.at[n], sf_r.at[n], tp=xside[n % 2])
+        return remote(stage.at[n], xr.at[xside[1 - leg(n)], spot(n)], sf_s.at[n], sf_r.at[n], tp=xside[leg(n)])
 
     def second_leg_recv(n):
-        return remote(stage.at[n], xr.at[opposite, spot(n)], sf_s.at[n], sf_r.at[n], tp=xside[n % 2])
+        return remote(stage.at[n], xr.at[opposite, spot(n)], sf_s.at[n], sf_r.at[n], tp=xside[leg(n)])
 
     def xd(k):
         return remote(dn.at[(x + k) % TP], ds.at[p, :, dcols(x)], xd_s.at[k - 1], xd_r.at[k - 1], tp=(x + k) % TP)
@@ -140,22 +144,22 @@
     def send_packed(k, _):
         @pl.when(k == 0)
         def _():
-            first_leg(0).start()
-            first_leg(1).start()
+            for n in order[:2]:
+                first_leg(n).start()
 
         e = jnp.where(k < 2, jnp.where(k == 0, xside[0], xside[1]), x)
         pack(e)
 
         @pl.when(k == 0)
         def _():
-            for n in range(Q):
+            for n in order:
                 xw(n, 0).start()
 
         @pl.when(k == 1)
         def _():
-            for n in range(Q):
+            for n in order:
                 xw(n, 1).start()
-            for n in range(2, Q):
+            for n in order[2:]:
                 first_leg(n).start()
 
         return 0
@@ -207,16 +211,20 @@
                 for way in (0, 1):
                     across(2 * s - 2 + side, fo, way).start()
 
-    turns = ((1, 3), (2, 0))
+    turns = (
+        ((0, 1), (0, 3)), ((0, 2), (0, 0)), ((2, 1), (2, 2)), ((2, 0), (2, 3)),
+        ((3, 1), (1, 2)), ((1, 1), (3, 2)), ((3, 0), (1, 3)), ((1, 0), (3, 3)),
+    )
+    needs = {0: (0,), 2: (2,), 4: (1, 3)}
 
     def za(n, u, cd):
-        zc = ((zone + u) % TP) * Q + spot(n)
+        zc = (z + n + Q * u) % Z
         return remote(
             xr.at[zc // Q, spot(n), cd], gu.at[f, p], za_s.at[n * TP + u, cd], za_r.at[n * TP + u, c], fs=zc * 2 + cd
         )
 
     def source(n, u):
-        return ((zone + TP - u) % TP) * Q + (seat + Q - n) % Q
+        return (z + Z - n - Q * u) % Z
 
     def za_recv(n, u, cs):
         held = gu.at[2 * source(n, u) + cs, p]
@@ -233,12 +241,11 @@
     own = pltpu.make_async_copy(xr.at[zone, seat, c], gu.at[f, p], loc.at[4])
 
     def issue(b):
-        n = b // 2
-        if b % 2 == 0:
+        for n in needs.get(b, ()):
             for side in (0, 1):
                 xw_recv(n, side).wait_recv()
             second_leg_recv(n).wait_recv()
-        for u in turns[b % 2]:
+        for n, u in turns[b]:
             if n == 0 and u == 0:
                 za(0, 0, 1 - c).start()
                 own.start()
@@ -247,8 +254,7 @@
                 za(n, u, 1).start()
 
     def accept(b):
-        n = b // 2
-        for u in turns[b % 2]:
+        for n, u in turns[b]:
             if n == 0 and u == 0:
                 own.wait()
                 za_recv(0, 0, 1 - c).wait_recv()
@@ -292,10 +298,7 @@
 
     yd = remote(ds.at[p], ds.at[p], yd_s, yd_r, grp=mate)
     ring_step(1)
-    for n in (0, 1):
-        first_leg(n).wait_recv()
-        second_leg(n).start()
-    for n in range(2, Q):
+    for n in order:
         first_leg(n).wait_recv()
         second_leg(n).start()
     for k in (2, 1, 3):
@@ -303,11 +306,10 @@
     ring_step(2)
     local[0].wait()
     issue(0)
+    issue(1)
     for s in range(3, H + 1):
         ring_step(s)
-        issue(s - 2)
-        if s == H:
-            issue(s - 1)
+        issue(s - 1)
         for i in (2 * s - 6, 2 * s - 5):
             pass_on(i)
         if s == 4:
@@ -443,7 +445,9 @@
     ])
 
 
-def unpack(block, gu, wg, wu, gate_out, up_out):
+def unpack(block, gu, ds, wg, wu, gate_out, up_out, down_out, sem):
+    down = pltpu.make_async_copy(ds, down_out, sem)
+    down.start()
     part, ff = gu.shape[2], gu.shape[3] // 4
     pieces = block // (2 * part)
 
@@ -461,9 +465,10 @@
         return 0
 
     lax.fori_loop(0, wg.shape[0] // block, step, 0)
-
-
-def run_unpack(gu):
+    down.wait()
+
+
+def run_unpack(gu, ds):
     ff = gu.shape[3] // 4
     features = gu.shape[0] * gu.shape[1] * gu.shape[2] * 2
     vmem = pl.BlockSpec(memory_space=pltpu.VMEM)
@@ -475,13 +480,15 @@
             jax.ShapeDtypeStruct((features, ff), bf16),
             jax.ShapeDtypeStruct((ff, features), bf16),
             jax.ShapeDtypeStruct((ff, features), bf16),
+            jax.ShapeDtypeStruct(ds.shape, bf16),
         ),
-        in_specs=[vmem],
-        out_specs=(vmem,) * 4,
+        in_specs=[vmem] * 2,
+        out_specs=(vmem,) * 4 + (pl.BlockSpec(memory_space=pltpu.HBM),),
+        scratch_shapes=[DMA],
         compiler_params=pltpu.CompilerParams(vmem_limit_bytes=8 << 20),
         cost_estimate=pl.CostEstimate(flops=10**9, bytes_accessed=16 << 20, transcendentals=0),
         name="unpack",
-    )(gu)
+    )(gu, ds)
 
 
 def combine(FS, TP, L, wg, wu, tok, wall, wd, out, wdt, hs, part, prec, zs, zr, outt, turned, xd_s, xd_r, xo_s, xo_r, cc_s, cc_r, z_s, z_r, fin_s, fin_r):
@@ -545,7 +552,7 @@
     def arrival(side, k):
         return remote(zs.at[0], zr.at[side, k], z_s.at[0], z_r.at[side, k], fs=zside[side])
 
-    AHEAD = 4
+    AHEAD = 2
 
     def begin(k, _):
         make(2 * k)
@@ -682,9 +689,9 @@
     gu, ds, tok, wall = run_hand_over(
         FS, TP, tokens, routes.T, route_logits.T, gain[None], w_gate, w_up, w_down
     )
-    wg, wu, gate_t, up_t = run_unpack(gu)
+    wg, wu, gate_t, up_t, down = run_unpack(gu, ds)
     mixed = run_combine(FS, TP, wg, wu, tok, wall, w_down)
-    return (gate_t.T[None], up_t.T[None], ds.reshape(1, 2 * ds.shape[1], -1), mixed)
+    return (gate_t.T[None], up_t.T[None], down.reshape(1, 2 * ds.shape[1], -1), mixed)
 
 
 def solution(mesh):

time: 155 us -> 153 us (0.987)
  no operation moved by 1% of the time
where the time goes in v7:
time: 153 us
  Pallas kernels  152 us (99%)
    pallas_call x1, Pallas kernels, run_hand_over(): pl.pallas_call(functools.partial(hand_over, FS, TP), out_shape=(jax.Shape...  99.9 us
    pallas_call x1, Pallas kernels, run_combine(): pl.pallas_call(functools.partial(combine, FS, TP, 2), out_shape=jax.Shape...  48.4 us
    pallas_call x1, Pallas kernels, run_unpack(): pl.pallas_call(functools.partial(unpack, 256), out_shape=(jax.ShapeDtypeS...  3.6 us

profile of v7, /device:TPU:33, one launch (start us, length us, event | category | flops | bytes accessed | tf_op | source)
XLA Modules:
  0.0 153.2 jit_solution(7073021520738637241)
XLA Ops:
  0.6 99.9 %hand_over.1 = (bf16[32,2,16,896]{3,2,1,0:T(8,128)(2,1)S(1)}, bf16[2,112,2048]{2,1,0:T(8,128)(2,1)S(1)}, bf16[32,64,2048]{2,1,0:T(8,128)(2,1)S(1)}, bf16[32,16,128]{2,1,0:T(8,128)(2,1)S(1)}) custom-call(bf16[64,2048]{1,0:T(8,128)(2,1)} %x_hbm.1, s32[2,64]{1,0:T(2,128)} %bitcast.10, f32[2,64]{1,0:T(2,128)} %bitcast.11, f32[1,64]{1,0:T(1,128)} %bitcast.12, ...), custom_call_target="tpu_custom_call" | custom-call | flops 1000000000 | bytes 31457280 | tf_op jit(solution)/shard_map/hand_over/pallas_call | solution.py:405
  100.5 0.0 copy-start
  100.5 3.6 %unpack.1 = (bf16[2048,224]{1,0:T(8,128)(2,1)S(1)}, bf16[2048,224]{1,0:T(8,128)(2,1)S(1)}, bf16[224,2048]{1,0:T(8,128)(2,1)}, bf16[224,2048]{1,0:T(8,128)(2,1)}, bf16[2,112,2048]{2,1,0:T(8,128)(2,1)}) custom-call(bf16[32,2,16,896]{3,2,1,0:T(8,128)(2,1)S(1)} %get-tuple-element.13.gu, bf16[2,112,2048]{2,1,0:T(8,128)(2,1)S(1)} %get-tuple-element.14.ds), custom_call_target="tpu_custom_call" | custom-call | flops 1000000000 | bytes 16777216 | tf_op jit(solution)/shard_map/unpack/pallas_call | solution.py:476
  104.2 0.0 copy-done
  104.2 48.4 %combine.1 = bf16[64,512]{1,0:T(8,128)(2,1)S(1)} custom-call(bf16[2048,224]{1,0:T(8,128)(2,1)S(1)} %get-tuple-element.18.wg, bf16[2048,224]{1,0:T(8,128)(2,1)S(1)} %get-tuple-element.19.wu, bf16[32,64,2048]{2,1,0:T(8,128)(2,1)S(1)} %get-tuple-element.20.tok, bf16[32,16,128]{2,1,0:T(8,128)(2,1)S(1)} %get-tuple-element.21.wall, f32[4,224,512]{2,1,0:T(8,128)S(1)} %copy-done), custom_call_target="tpu_custom_call" | custom-call | flops 1000000000 | bytes 31457280 | tf_op jit(solution)/shard_map/combine/pallas_call | solution.py:665
  152.5 0.6 copy.12
Async XLA Ops:
  100.5 3.6 %copy-start = (f32[4,224,512]{2,1,0:T(8,128)S(1)}, f32[4,224,512]{2,1,0:T(8,128)}, u32[]{:S(2)}) copy-start(f32[4,224,512]{2,1,0:T(8,128)} %wd.1) | copy-start | bytes 5505028

commit v8 on v7

--- a/solution.py
+++ b/solution.py
@@ -320,12 +320,11 @@
         if s > 3:
             for i in (2 * s - 8, 2 * s - 7):
                 finish(i)
-            accept(s - 4)
+        accept(s - 3)
     pass_on(2 * H - 4)
     pass_on(2 * H - 3)
     finish(2 * H - 6)
     finish(2 * H - 5)
-    accept(H - 3)
     pass_on(2 * H - 2)
     finish(2 * H - 4)
     finish(2 * H - 3)
@@ -445,11 +444,17 @@
     ])
 
 
-def unpack(block, gu, ds, wg, wu, gate_out, up_out, down_out, sem):
+def unpack(block, gu, ds, wg, wu, gate_out, up_out, down_out, gate_t, up_t, sem, sems):
     down = pltpu.make_async_copy(ds, down_out, sem)
     down.start()
     part, ff = gu.shape[2], gu.shape[3] // 4
     pieces = block // (2 * part)
+    blocks = wg.shape[0] // block
+
+    def served(i, n):
+        span = pl.ds(pl.multiple_of(i * block, block), block)
+        held, out = ((gate_t, gate_out), (up_t, up_out))[n]
+        return pltpu.make_async_copy(held.at[:, span], out.at[:, span], sems.at[n, i])
 
     def step(i, _):
         span = pl.ds(pl.multiple_of(i * block, block), block)
@@ -460,12 +465,20 @@
                 at = pl.ds(pl.multiple_of(k * 2 * part + hh * part, part), part)
                 wg[at, :] = piece[:, 2 * hh * ff : (2 * hh + 1) * ff].astype(jnp.bfloat16)
                 wu[at, :] = piece[:, (2 * hh + 1) * ff : (2 * hh + 2) * ff].astype(jnp.bfloat16)
-        for own, served in ((wg, gate_out), (wu, up_out)):
-            served[:, span] = own[span, :].astype(jnp.float32).T.astype(jnp.bfloat16)
-        return 0
-
-    lax.fori_loop(0, wg.shape[0] // block, step, 0)
+        for n, (own, held) in enumerate(((wg, gate_t), (wu, up_t))):
+            held[:, span] = own[span, :].astype(jnp.float32).T.astype(jnp.bfloat16)
+            served(i, n).start()
+        return 0
+
+    lax.fori_loop(0, blocks, step, 0)
     down.wait()
+
+    def drain(i, _):
+        served(i, 0).wait()
+        served(i, 1).wait()
+        return 0
+
+    lax.fori_loop(0, blocks, drain, 0)
 
 
 def run_unpack(gu, ds):
@@ -483,8 +496,10 @@
             jax.ShapeDtypeStruct(ds.shape, bf16),
         ),
         in_specs=[vmem] * 2,
-        out_specs=(vmem,) * 4 + (pl.BlockSpec(memory_space=pltpu.HBM),),
-        scratch_shapes=[DMA],
+        out_specs=(vmem,) * 2 + (pl.BlockSpec(memory_space=pltpu.HBM),) * 3,
+        scratch_shapes=[
+            pltpu.VMEM((ff, features), bf16), pltpu.VMEM((ff, features), bf16), DMA, DMA((2, features // 256)),
+        ],
         compiler_params=pltpu.CompilerParams(vmem_limit_bytes=8 << 20),
         cost_estimate=pl.CostEstimate(flops=10**9, bytes_accessed=16 << 20, transcendentals=0),
         name="unpack",

time: 153 us -> 153 us (level)
  no operation moved by 1% of the time
where the time goes in v8:
time: 153 us
  Pallas kernels  152 us (99%)
    pallas_call x1, Pallas kernels, run_hand_over(): pl.pallas_call(functools.partial(hand_over, FS, TP), out_shape=(jax.Shape...  99.8 us
    pallas_call x1, Pallas kernels, run_combine(): pl.pallas_call(functools.partial(combine, FS, TP, 2), out_shape=jax.Shape...  48.5 us
    pallas_call x1, Pallas kernels, run_unpack(): pl.pallas_call(functools.partial(unpack, 256), out_shape=(jax.ShapeDtypeS...  3.24 us

profile of v8, /device:TPU:33, one launch (start us, length us, event | category | flops | bytes accessed | tf_op | source)
XLA Modules:
  0.0 152.9 jit_solution(14475211484855314373)
XLA Ops:
  0.6 99.8 %hand_over.1 = (bf16[32,2,16,896]{3,2,1,0:T(8,128)(2,1)S(1)}, bf16[2,112,2048]{2,1,0:T(8,128)(2,1)S(1)}, bf16[32,64,2048]{2,1,0:T(8,128)(2,1)S(1)}, bf16[32,16,128]{2,1,0:T(8,128)(2,1)S(1)}) custom-call(bf16[64,2048]{1,0:T(8,128)(2,1)} %x_hbm.1, s32[2,64]{1,0:T(2,128)} %bitcast.10, f32[2,64]{1,0:T(2,128)} %bitcast.11, f32[1,64]{1,0:T(1,128)} %bitcast.12, ...), custom_call_target="tpu_custom_call" | custom-call | flops 1000000000 | bytes 31457280 | tf_op jit(solution)/shard_map/hand_over/pallas_call | solution.py:404
  100.5 0.0 copy-start
  100.5 3.2 %unpack.1 = (bf16[2048,224]{1,0:T(8,128)(2,1)S(1)}, bf16[2048,224]{1,0:T(8,128)(2,1)S(1)}, bf16[224,2048]{1,0:T(8,128)(2,1)}, bf16[224,2048]{1,0:T(8,128)(2,1)}, bf16[2,112,2048]{2,1,0:T(8,128)(2,1)}) custom-call(bf16[32,2,16,896]{3,2,1,0:T(8,128)(2,1)S(1)} %get-tuple-element.13.gu, bf16[2,112,2048]{2,1,0:T(8,128)(2,1)S(1)} %get-tuple-element.14.ds), custom_call_target="tpu_custom_call" | custom-call | flops 1000000000 | bytes 16777216 | tf_op jit(solution)/shard_map/unpack/pallas_call | solution.py:489
  103.7 0.0 copy-done
  103.7 48.5 %combine.1 = bf16[64,512]{1,0:T(8,128)(2,1)S(1)} custom-call(bf16[2048,224]{1,0:T(8,128)(2,1)S(1)} %get-tuple-element.18.wg, bf16[2048,224]{1,0:T(8,128)(2,1)S(1)} %get-tuple-element.19.wu, bf16[32,64,2048]{2,1,0:T(8,128)(2,1)S(1)} %get-tuple-element.20.tok, bf16[32,16,128]{2,1,0:T(8,128)(2,1)S(1)} %get-tuple-element.21.wall, f32[4,224,512]{2,1,0:T(8,128)S(1)} %copy-done), custom_call_target="tpu_custom_call" | custom-call | flops 1000000000 | bytes 31457280 | tf_op jit(solution)/shard_map/combine/pallas_call | solution.py:680
  152.3 0.6 copy.12
Async XLA Ops:
  100.5 3.3 %copy-start = (f32[4,224,512]{2,1,0:T(8,128)S(1)}, f32[4,224,512]{2,1,0:T(8,128)}, u32[]{:S(2)}) copy-start(f32[4,224,512]{2,1,0:T(8,128)} %wd.1) | copy-start | bytes 5505028

commit v9 on v8

--- a/solution.py
+++ b/solution.py
@@ -298,14 +298,17 @@
 
     yd = remote(ds.at[p], ds.at[p], yd_s, yd_r, grp=mate)
     ring_step(1)
-    for n in order:
+    for n in order[:2]:
+        first_leg(n).wait_recv()
+        second_leg(n).start()
+    local[0].wait()
+    issue(0)
+    ring_step(2)
+    for n in order[2:]:
         first_leg(n).wait_recv()
         second_leg(n).start()
     for k in (2, 1, 3):
         xd(k).start()
-    ring_step(2)
-    local[0].wait()
-    issue(0)
     issue(1)
     for s in range(3, H + 1):
         ring_step(s)

time: 153 us -> 155 us (1.013)
    pallas_call x1, Pallas kernels: 99.8 us -> 102 us  [run_hand_over(): pl.pallas_call(functools.partial(hand_over, FS, TP), out_shape=(jax.Shape...]
where the time goes in v9:
time: 155 us
  Pallas kernels  153 us (99%)
    pallas_call x1, Pallas kernels, run_hand_over(): pl.pallas_call(functools.partial(hand_over, FS, TP), out_shape=(jax.Shape...  102 us
    pallas_call x1, Pallas kernels, run_combine(): pl.pallas_call(functools.partial(combine, FS, TP, 2), out_shape=jax.Shape...  47.6 us
    pallas_call x1, Pallas kernels, run_unpack(): pl.pallas_call(functools.partial(unpack, 256), out_shape=(jax.ShapeDtypeS...  3.24 us

profile of v9, /device:TPU:33, one launch (start us, length us, event | category | flops | bytes accessed | tf_op | source)
XLA Modules:
  0.0 154.6 jit_solution(6502221324966849917)
XLA Ops:
  0.6 102.5 %hand_over.1 = (bf16[32,2,16,896]{3,2,1,0:T(8,128)(2,1)S(1)}, bf16[2,112,2048]{2,1,0:T(8,128)(2,1)S(1)}, bf16[32,64,2048]{2,1,0:T(8,128)(2,1)S(1)}, bf16[32,16,128]{2,1,0:T(8,128)(2,1)S(1)}) custom-call(bf16[64,2048]{1,0:T(8,128)(2,1)} %x_hbm.1, s32[2,64]{1,0:T(2,128)} %bitcast.10, f32[2,64]{1,0:T(2,128)} %bitcast.11, f32[1,64]{1,0:T(1,128)} %bitcast.12, ...), custom_call_target="tpu_custom_call" | custom-call | flops 1000000000 | bytes 31457280 | tf_op jit(solution)/shard_map/hand_over/pallas_call | solution.py:407
  103.1 0.0 copy-start
  103.1 3.2 %unpack.1 = (bf16[2048,224]{1,0:T(8,128)(2,1)S(1)}, bf16[2048,224]{1,0:T(8,128)(2,1)S(1)}, bf16[224,2048]{1,0:T(8,128)(2,1)}, bf16[224,2048]{1,0:T(8,128)(2,1)}, bf16[2,112,2048]{2,1,0:T(8,128)(2,1)}) custom-call(bf16[32,2,16,896]{3,2,1,0:T(8,128)(2,1)S(1)} %get-tuple-element.13.gu, bf16[2,112,2048]{2,1,0:T(8,128)(2,1)S(1)} %get-tuple-element.14.ds), custom_call_target="tpu_custom_call" | custom-call | flops 1000000000 | bytes 16777216 | tf_op jit(solution)/shard_map/unpack/pallas_call | solution.py:492
  106.4 0.0 copy-done
  106.4 47.6 %combine.1 = bf16[64,512]{1,0:T(8,128)(2,1)S(1)} custom-call(bf16[2048,224]{1,0:T(8,128)(2,1)S(1)} %get-tuple-element.18.wg, bf16[2048,224]{1,0:T(8,128)(2,1)S(1)} %get-tuple-element.19.wu, bf16[32,64,2048]{2,1,0:T(8,128)(2,1)S(1)} %get-tuple-element.20.tok, bf16[32,16,128]{2,1,0:T(8,128)(2,1)S(1)} %get-tuple-element.21.wall, f32[4,224,512]{2,1,0:T(8,128)S(1)} %copy-done), custom_call_target="tpu_custom_call" | custom-call | flops 1000000000 | bytes 31457280 | tf_op jit(solution)/shard_map/combine/pallas_call | solution.py:683
  154.0 0.6 copy.12
Async XLA Ops:
  103.1 3.3 %copy-start = (f32[4,224,512]{2,1,0:T(8,128)S(1)}, f32[4,224,512]{2,1,0:T(8,128)}, u32[]{:S(2)}) copy-start(f32[4,224,512]{2,1,0:T(8,128)} %wd.1) | copy-start | bytes 5505028

commit v10 on v8

--- a/solution.py
+++ b/solution.py
@@ -678,7 +678,7 @@
     feats = wd.shape[2]
     vmem = pl.BlockSpec(memory_space=pltpu.VMEM)
     return pl.pallas_call(
-        functools.partial(combine, FS, TP, 2),
+        functools.partial(combine, FS, TP, 3),
         out_shape=jax.ShapeDtypeStruct((block // 2, feats), jnp.bfloat16),
         in_specs=[vmem] * 5,
         out_specs=vmem,

time: 153 us -> 155 us (1.013)
    pallas_call x1, Pallas kernels: 48.5 us -> 50.3 us  [run_combine(): pl.pallas_call(functools.partial(combine, FS, TP, 3), out_shape=jax.Shape...]
where the time goes in v10:
time: 155 us
  Pallas kernels  153 us (99%)
    pallas_call x1, Pallas kernels, run_hand_over(): pl.pallas_call(functools.partial(hand_over, FS, TP), out_shape=(jax.Shape...  99.8 us
    pallas_call x1, Pallas kernels, run_combine(): pl.pallas_call(functools.partial(combine, FS, TP, 3), out_shape=jax.Shape...  50.3 us
    pallas_call x1, Pallas kernels, run_unpack(): pl.pallas_call(functools.partial(unpack, 256), out_shape=(jax.ShapeDtypeS...  3.24 us

profile of v10, /device:TPU:33, one launch (start us, length us, event | category | flops | bytes accessed | tf_op | source)
XLA Modules:
  0.0 154.7 jit_solution(11486592540585651224)
XLA Ops:
  0.6 99.8 %hand_over.1 = (bf16[32,2,16,896]{3,2,1,0:T(8,128)(2,1)S(1)}, bf16[2,112,2048]{2,1,0:T(8,128)(2,1)S(1)}, bf16[32,64,2048]{2,1,0:T(8,128)(2,1)S(1)}, bf16[32,16,128]{2,1,0:T(8,128)(2,1)S(1)}) custom-call(bf16[64,2048]{1,0:T(8,128)(2,1)} %x_hbm.1, s32[2,64]{1,0:T(2,128)} %bitcast.10, f32[2,64]{1,0:T(2,128)} %bitcast.11, f32[1,64]{1,0:T(1,128)} %bitcast.12, ...), custom_call_target="tpu_custom_call" | custom-call | flops 1000000000 | bytes 31457280 | tf_op jit(solution)/shard_map/hand_over/pallas_call | solution.py:404
  100.5 0.0 copy-start
  100.5 3.2 %unpack.1 = (bf16[2048,224]{1,0:T(8,128)(2,1)S(1)}, bf16[2048,224]{1,0:T(8,128)(2,1)S(1)}, bf16[224,2048]{1,0:T(8,128)(2,1)}, bf16[224,2048]{1,0:T(8,128)(2,1)}, bf16[2,112,2048]{2,1,0:T(8,128)(2,1)}) custom-call(bf16[32,2,16,896]{3,2,1,0:T(8,128)(2,1)S(1)} %get-tuple-element.13.gu, bf16[2,112,2048]{2,1,0:T(8,128)(2,1)S(1)} %get-tuple-element.14.ds), custom_call_target="tpu_custom_call" | custom-call | flops 1000000000 | bytes 16777216 | tf_op jit(solution)/shard_map/unpack/pallas_call | solution.py:489
  103.7 0.0 copy-done
  103.7 50.3 %combine.1 = bf16[64,512]{1,0:T(8,128)(2,1)S(1)} custom-call(bf16[2048,224]{1,0:T(8,128)(2,1)S(1)} %get-tuple-element.18.wg, bf16[2048,224]{1,0:T(8,128)(2,1)S(1)} %get-tuple-element.19.wu, bf16[32,64,2048]{2,1,0:T(8,128)(2,1)S(1)} %get-tuple-element.20.tok, bf16[32,16,128]{2,1,0:T(8,128)(2,1)S(1)} %get-tuple-element.21.wall, f32[4,224,512]{2,1,0:T(8,128)S(1)} %copy-done), custom_call_target="tpu_custom_call" | custom-call | flops 1000000000 | bytes 31457280 | tf_op jit(solution)/shard_map/combine/pallas_call | solution.py:680
  154.1 0.6 copy.12
Async XLA Ops:
  100.5 3.3 %copy-start = (f32[4,224,512]{2,1,0:T(8,128)S(1)}, f32[4,224,512]{2,1,0:T(8,128)}, u32[]{:S(2)}) copy-start(f32[4,224,512]{2,1,0:T(8,128)} %wd.1) | copy-start | bytes 5505028
